TPU v7x, 32 devices: a whole 2x2x4 slice. The times are simulated.
32 devices in a mesh: kv: 8 (over z, x), tp: 4 (over y, core).
Axes of the slice: x: 2, y: 2, z: 4, core: 2. Of those that a mesh axis runs over, the one named last changes fastest.
Arguments:
- tokens: bfloat16 [4096, 2048], P(('kv', 'tp')), may hold values from -6 to 6
- query_weight: bfloat16 [2048, 1024], P(None, 'tp'), may hold values from -0.125 to 0.125
- latent_weight: bfloat16 [2048, 256], replicated, may hold values from -0.125 to 0.125
- key_absorb: bfloat16 [8, 128, 256], P('tp'), may hold values from -0.5 to 0.5
- query_gain: bfloat16 [256], replicated, may hold values from 0.4 to 8
- latent_gain: bfloat16 [256], replicated, may hold values from 0.4 to 8
- value_absorb: bfloat16 [8, 256, 128], P('tp'), may hold values from -0.375 to 0.375
- head_gain: bfloat16 [8, 128], P('tp'), may hold values from 0.099609375 to 1.8984375
- out_weight: bfloat16 [1024, 2048], P('tp'), may hold values from -0.1875 to 0.1875
- chosen: int32 [64, 11], P('kv'), may hold values from 0 to 63, as said below
Outputs:
- mixed_out: bfloat16 [4096, 2048], P(('kv', 'tp'))
Inputs may be any that keep to these rules, and one draw needn't show every extreme that they name: `chosen`: entry 0 of row b is b; a row's entries are distinct. Entries 1 to 3 lie in the same aligned run of 8 block numbers as b, the other 7 in other runs. For each aligned run of 8 rows and each other aligned run of 8 block numbers, those rows together name at most one block of that run. Entries above the row's own number may occur and contribute nothing.
All inputs are finite; a program needn't handle non-finite values.
Results may differ from a plain program's by a relative error of at most 0.014.
The roundings to bfloat16 on the way count: a program that leaves them out, or rounds other values in their place, can miss the bound.
Values may be sent and summed in bfloat16 or wider, within the bound.
No kernel may reach another device: no remote copies, remote signals or barrier semaphores. Data moves between devices by JAX's collectives and lax.ppermute only.
A program may use at most 64 MiB of HBM per device.

v0:
```python
import jax
import jax.numpy as jnp
from jax import lax
from jax.sharding import PartitionSpec as P

epsilon = 1e-06


def normalize(values, gain):
    return values * lax.rsqrt(jnp.mean(values * values, axis=-1, keepdims=True) + epsilon) * gain


def body(
    tokens,
    query_weight,
    latent_weight,
    key_absorb,
    query_gain,
    latent_gain,
    value_absorb,
    head_gain,
    out_weight,
    chosen,
):
    width_query = query_weight.shape[1]
    shard_rows = lax.all_gather(tokens, "tp", axis=0, tiled=True)
    query_part = jnp.dot(shard_rows, query_weight, preferred_element_type=jnp.float32)
    latent_part = jnp.dot(shard_rows, latent_weight, preferred_element_type=jnp.float32)
    projected = jnp.concatenate([query_part, latent_part], axis=1)
    local_heads, head_width, latent_width = key_absorb.shape
    span_tokens = projected.shape[0]
    queries = (
        projected[:, :width_query]
        .astype(jnp.bfloat16)
        .reshape(span_tokens, local_heads, head_width)
    )
    latent = normalize(projected[:, width_query:], latent_gain.astype(jnp.float32)).astype(
        jnp.bfloat16
    )
    absorbed = jnp.einsum("thd,hdc->thc", queries, key_absorb, preferred_element_type=jnp.float32)
    absorbed = normalize(absorbed, query_gain.astype(jnp.float32)).astype(jnp.bfloat16)
    block_count, pick_count = chosen.shape
    block_len = span_tokens // block_count
    devices = lax.axis_size("kv")
    own_index = lax.axis_index("kv")
    owner_of = chosen // block_count
    within = chosen % block_count
    device_ids = jnp.arange(devices, dtype=jnp.int32)
    matches = owner_of[:, :, None] == device_ids[None, None, :]
    wanted = jnp.max(jnp.where(matches, within[:, :, None], 0), axis=(0, 1))
    asked_for = lax.all_to_all(wanted, "kv", split_axis=0, concat_axis=0, tiled=True)
    blocks = latent.reshape(block_count, block_len, latent_width)
    outgoing = jnp.take(blocks, asked_for, axis=0)
    arrived = lax.all_to_all(outgoing, "kv", split_axis=0, concat_axis=0, tiled=True)
    key_table = jnp.concatenate([blocks, arrived], axis=0)
    table_slot = jnp.where(owner_of == own_index, within, block_count + owner_of)
    key_rows = jnp.take(key_table, table_slot, axis=0).reshape(
        block_count, pick_count * block_len, latent_width
    )
    offsets = jnp.arange(block_len, dtype=jnp.int32)
    key_pos = (chosen[:, :, None] * block_len + offsets[None, None, :]).reshape(
        block_count, pick_count * block_len
    )
    block_ids = own_index * block_count + jnp.arange(block_count, dtype=jnp.int32)
    query_pos = block_ids[:, None] * block_len + offsets[None, :]
    visible = key_pos[:, None, :] <= query_pos[:, :, None]
    grouped = absorbed.reshape(block_count, block_len, local_heads, latent_width)
    scores = jnp.einsum(
        "bqhc,bkc->bhqk", grouped, key_rows, preferred_element_type=jnp.float32
    ) * latent_width ** (-0.5)
    scores = jnp.where(visible[:, None], scores, -jnp.inf)
    weights = jax.nn.softmax(scores, axis=-1).astype(jnp.bfloat16)
    mixed = jnp.einsum(
        "bhqk,bkc->bqhc", weights, key_rows, preferred_element_type=jnp.float32
    ).astype(jnp.bfloat16)
    mixed = mixed.reshape(span_tokens, local_heads, latent_width)
    values = jnp.einsum("thc,hcd->thd", mixed, value_absorb, preferred_element_type=jnp.float32)
    head_out = (
        normalize(values, head_gain.astype(jnp.float32))
        .astype(jnp.bfloat16)
        .reshape(span_tokens, local_heads * head_width)
    )
    return lax.psum_scatter(
        jnp.dot(head_out, out_weight, preferred_element_type=jnp.float32).astype(jnp.bfloat16),
        "tp",
        scatter_dimension=0,
        tiled=True,
    )


def solution(mesh):
    return jax.shard_map(
        body,
        mesh=mesh,
        in_specs=(
            P(("kv", "tp"), None),
            P(None, "tp"),
            P(),
            P("tp", None, None),
            P(),
            P(),
            P("tp", None, None),
            P("tp", None),
            P("tp", None),
            P("kv", None),
        ),
        out_specs=P(("kv", "tp"), None),
        check_vma=False,
    )
```

profile of v0, /device:TPU:0, one launch (start us, length us, event | category | flops | bytes accessed | tf_op | source)
XLA Modules:
  0.0 101.6 jit_solution(10728988951733856679)
XLA Ops:
  6.5 0.7 all-gather.2.cloned.1.call-update
  7.3 0.7 broadcast_multiply_fusion
  8.1 0.7 copy.28
  8.8 7.3 %all-to-all-start = ((s32[8,1,1]{2,1,0:T(1,128)}), s32[8,1,1]{2,1,0:T(1,128)S(1)}, u32[]{:S(2)}, u32[]{:S(2)}) async-start(s32[8,1,1]{2,1,0:T(1,128)} %copy.28), calls=%async_computation | async-start | bytes 8192 | tf_op jit(solution)/shard_map/all_to_all | solution.py:51
  16.0 0.7 convert_element_type.33
  16.7 0.7 compare_and_fusion
  17.7 0.7 convert_element_type.36
  19.0 0.7 convert_element_type.41
  19.6 2.8 %all-to-all-done = s32[8,1,1]{2,1,0:T(1,128)S(1)} async-done(((s32[8,1,1]{2,1,0:T(1,128)}), s32[8,1,1]{2,1,0:T(1,128)S(1)}, u32[]{:S(2)}, u32[]{:S(2)}) %all-to-all-start) | async-done | bytes 64 | tf_op jit(solution)/shard_map/all_to_all | solution.py:51
  22.7 11.5 %all-gather.2.cloned.1.call-done = bf16[512,2048]{1,0:T(8,128)(2,1)} async-done(((bf16[128,2048]{1,0:T(8,128)(2,1)}), bf16[512,2048]{1,0:T(8,128)(2,1)}) %all-gather.2.cloned.1.call-update) | async-done | bytes 2097168 | tf_op jit(solution)/shard_map/all_gather | solution.py:26
  34.2 2.6 %multiply_reduce_fusion.2 = (f32[512]{0:T(512)S(1)}, f32[512,256]{1,0:T(8,128)S(1)}) fusion(bf16[512,2048]{1,0:T(8,128)(2,1)} %all-gather.2.cloned.1.call-done, bf16[2048,256]{1,0:T(8,128)(2,1)} %param.12), kind=kOutput, calls=%fused_computation.29 | convolution fusion | flops 537132544 | bytes 3672064 | tf_op jit(solution)/shard_map/dot_general | solution.py:28
  37.0 0.6 gather_fusion
  37.6 0.8 broadcast_select_fusion
  38.4 5.5 %all-to-all-start.1 = ((bf16[8,64,256]{2,1,0:T(8,128)(2,1)}), bf16[8,64,256]{2,1,0:T(8,128)(2,1)S(1)}, u32[]{:S(2)}, u32[]{:S(2)}) async-start(bf16[8,64,256]{2,1,0:T(8,128)(2,1)} %broadcast_select_fusion), calls=%async_computation.1 | async-start | bytes 524288 | tf_op jit(solution)/shard_map/all_to_all | solution.py:54
  44.0 2.4 %convolution_convert_fusion.1 = bf16[512,256]{0,1:T(8,128)(2,1)S(1)} fusion(bf16[512,2048]{1,0:T(8,128)(2,1)} %all-gather.2.cloned.1.call-done, bf16[2048,256]{1,0:T(8,128)(2,1)S(1)} %copy-done.3), kind=kOutput, calls=%fused_computation.20 | convolution fusion | flops 537001984 | bytes 3407872 | tf_op jit(solution)/shard_map/dot_general | solution.py:27
  46.3 0.5 multiply_reduce_fusion
  47.0 6.2 %all-to-all-done.1 = bf16[8,64,256]{2,1,0:T(8,128)(2,1)S(1)} async-done(((bf16[8,64,256]{2,1,0:T(8,128)(2,1)}), bf16[8,64,256]{2,1,0:T(8,128)(2,1)S(1)}, u32[]{:S(2)}, u32[]{:S(2)}) %all-to-all-start.1) | async-done | bytes 262176 | tf_op jit(solution)/shard_map/all_to_all | solution.py:54
  53.3 2.5 %gather_fusion.1 = bf16[88,64,256]{2,1,0:T(8,128)(2,1)} fusion(bf16[16,64,256]{2,1,0:T(8,128)(2,1)S(1)} %pad_maximum_fusion, s32[1024]{0:T(1024)S(1)} %pad_clamp_fusion), kind=kCustom, calls=%fused_computation.1 | custom fusion | bytes 5767520 | tf_op jit(solution)/shard_map/jit(_take)/gather | solution.py:57
  55.7 3.2 %bitcast_select_fusion.1 = bf16[8,704,256]{2,1,0:T(8,128)(2,1)S(1)} fusion(pred[8,704]{1,0:T(8,128)(4,1)S(1)} %broadcast_in_dim.68, bf16[8,704,256]{2,1,0:T(8,128)(2,1)} %bitcast.51), kind=kLoop, calls=%fused_computation.11 | loop fusion | flops 1441792 | bytes 5772800 | tf_op jit(solution)/shard_map/jit(_take)/select_n | solution.py:57
  59.0 1.0 %fusion.3 = f32[8,704,64,2]{1,2,3,0:T(8,128)S(1)} fusion(bf16[8,704,256]{2,1,0:T(8,128)(2,1)S(1)} %bitcast_select_fusion.1, bf16[8,64,2,256]{3,1,0,2:T(8,128)(2,1)S(1)} %bitcast.54), kind=kOutput, calls=%fused_computation.9 | convolution fusion | flops 369098752 | bytes 6291456 | tf_op jit(solution)/shard_map/bqhc,bkc->bhqk/dot_general | solution.py:68
  60.0 1.8 %fusion.21 = (f32[8,2,64]{2,1,0:T(2,128)S(1)}, f32[8,2,64,704]{3,2,1,0:T(8,128)S(1)}) fusion(f32[8,704,64,2]{1,2,3,0:T(8,128)S(1)} %fusion.3, pred[8,64,704]{2,1,0:T(8,128)(4,1)S(1)} %broadcast_compare_fusion), kind=kOutput, calls=%fused_computation.58 | output fusion | flops 4326079 | bytes 6131712 | tf_op jit(solution)/shard_map/sub | solution.py:72
  61.9 0.7 fusion.12
  63.2 2.1 %convolution_convert_fusion = bf16[512,2048]{1,0:T(8,128)(2,1)} fusion(bf16[512,256]{0,1:T(8,128)(2,1)S(1)} %bitcast.56, bf16[256,2048]{1,0:T(8,128)(2,1)S(1)} %copy-done), kind=kOutput, calls=%fused_computation.6 | convolution fusion | flops 537919488 | bytes 3407872 | tf_op jit(solution)/shard_map/dot_general | solution.py:84
  65.4 29.4 %reduce-scatter.2.cloned.1.call-done = bf16[128,2048]{1,0:T(8,128)(2,1)} async-done(((bf16[512,2048]{1,0:T(8,128)(2,1)}), bf16[128,2048]{1,0:T(8,128)(2,1)}) %reduce-scatter.2.cloned.1.call-update) | async-done | bytes 524304 | tf_op jit(solution)/shard_map/reduce_scatter | solution.py:83
  (37 shorter events, 2.4 us)
Async XLA Ops:
  6.5 56.7 %copy-start = (bf16[256,2048]{1,0:T(8,128)(2,1)S(1)}, bf16[256,2048]{1,0:T(8,128)(2,1)}, u32[]{:S(2)}) copy-start(bf16[256,2048]{1,0:T(8,128)(2,1)} %param.18) | copy-start | bytes 3145732
  6.5 27.7 %all-gather.2.cloned.1.call-start = ((), (), s32[]{:S(2)}) async-start(), calls=%async_computation.3 | async-start | bytes 2621440 | tf_op jit(solution)/shard_map/all_gather | solution.py:26
  8.8 13.7 %all-to-all-start = ((s32[8,1,1]{2,1,0:T(1,128)}), s32[8,1,1]{2,1,0:T(1,128)S(1)}, u32[]{:S(2)}, u32[]{:S(2)}) async-start(s32[8,1,1]{2,1,0:T(1,128)} %copy.28), calls=%async_computation | async-start | bytes 8192 | tf_op jit(solution)/shard_map/all_to_all | solution.py:51
  22.7 21.2 %copy-start.3 = (bf16[2048,256]{1,0:T(8,128)(2,1)S(1)}, bf16[2048,256]{1,0:T(8,128)(2,1)}, u32[]{:S(2)}) copy-start(bf16[2048,256]{1,0:T(8,128)(2,1)} %param.11) | copy-start | bytes 3145732
  36.9 9.5 %copy-start.2 = (bf16[2,128,256]{2,1,0:T(8,128)(2,1)S(1)}, bf16[2,128,256]{2,1,0:T(8,128)(2,1)}, u32[]{:S(2)}) copy-start(bf16[2,128,256]{2,1,0:T(8,128)(2,1)} %param.13) | copy-start | bytes 393220
  38.4 14.8 %all-to-all-start.1 = ((bf16[8,64,256]{2,1,0:T(8,128)(2,1)}), bf16[8,64,256]{2,1,0:T(8,128)(2,1)S(1)}, u32[]{:S(2)}, u32[]{:S(2)}) async-start(bf16[8,64,256]{2,1,0:T(8,128)(2,1)} %broadcast_select_fusion), calls=%async_computation.1 | async-start | bytes 524288 | tf_op jit(solution)/shard_map/all_to_all | solution.py:54
  43.9 50.9 %reduce-scatter.2.cloned.1.call-start = ((), (), s32[]{:S(2)}) async-start(), calls=%async_computation.4 | async-start | bytes 2621440 | tf_op jit(solution)/shard_map/reduce_scatter | solution.py:83
  61.9 0.9 copy-start.1
Sparse Core Ops, SparseCore 0:
  8.9 25.2 all-gather.1
  65.5 29.2 reduce-scatter.1
where the time goes:
time: 102 us
  waiting for transfers between devices  50.6 us (50%)
  between operations  13.6 us (13%)
  starting transfers between devices  12.8 us (13%)
  other arithmetic  10.6 us (10%)
  matrix products  9.61 us (9%)
  local copies, waits for them, and re-layouts  4.43 us (4%)
    reduce_scatter x1, waiting for transfers between devices, body(): lax.psum_scatter(jnp.dot(head_out, out_weight, preferred_element_type=jnp...  29.4 us
    all_gather x1, waiting for transfers between devices, body(): shard_rows = lax.all_gather(tokens, 'tp', axis=0, tiled=True)  11.5 us
    all_to_all x1, starting transfers between devices, body(): lax.all_to_all(wanted, 'kv', split_axis=0, concat_axis=0, tiled=True)  7.28 us
    all_to_all x1, waiting for transfers between devices, body(): lax.all_to_all(outgoing, 'kv', split_axis=0, concat_axis=0, tiled=True)  6.18 us
    all_to_all x1, starting transfers between devices, body(): lax.all_to_all(outgoing, 'kv', split_axis=0, concat_axis=0, tiled=True)  5.51 us
    select_n x1, other arithmetic, body(): jnp.take(key_table, table_slot, axis=0)  3.22 us
    all_to_all x1, waiting for transfers between devices, body(): lax.all_to_all(wanted, 'kv', split_axis=0, concat_axis=0, tiled=True)  2.82 us
    dot_general x1, matrix products, body(): jnp.dot(shard_rows, latent_weight, preferred_element_type=jnp.float32)  2.65 us
  transfers between devices with their start and end apart: 4, of which 4 were waited for; matrix products, arithmetic and copies ran while one was open for 8% of the time, Pallas kernels for 0%

commit v1 on v0

v1 whole, which is shorter than its diff:
```python
import functools

import jax
import jax.numpy as jnp
from jax import lax
from jax.experimental import pallas as pl
from jax.experimental.pallas import tpu as pltpu
from jax.sharding import PartitionSpec as P


epsilon = 1e-06
f32 = jnp.float32
bf16 = jnp.bfloat16
VMEM = pl.BlockSpec(memory_space=pltpu.VMEM)
SMEM = pl.BlockSpec(memory_space=pltpu.SMEM)


def rms(values, gain):
    return values * lax.rsqrt(jnp.mean(values * values, axis=-1, keepdims=True) + epsilon) * gain


def call(kernel, out_shape, in_specs, scratch=(), flops=0, moved=0, out_specs=None):
    many = isinstance(out_shape, (list, tuple))
    return pl.pallas_call(
        kernel,
        out_shape=out_shape,
        in_specs=in_specs,
        out_specs=out_specs or ([VMEM] * len(out_shape) if many else VMEM),
        scratch_shapes=list(scratch),
        cost_estimate=pl.CostEstimate(flops=flops, bytes_accessed=moved, transcendentals=0),
    )


def latent_kernel(tokens, weight, gain, out):
    product = jnp.dot(tokens[...], weight[...], preferred_element_type=f32)
    out[...] = rms(product, gain[...].astype(f32)).astype(bf16)


def pick_kernel(per_shard, asked, own, core, far, diag, table, outgoing):
    me = lax.axis_index("tp")
    rows = own.shape[0]
    block_len = rows // per_shard
    table[pl.ds(0, rows)] = own[...]
    table[pl.ds(rows, rows)] = core[...]
    table[pl.ds(2 * rows, rows)] = far[...]
    table[pl.ds(3 * rows, rows)] = diag[...]

    def one(index, carry):
        within = asked[index]
        slot = jnp.bitwise_xor(within // per_shard, me) * per_shard + within % per_shard
        source = pl.multiple_of(slot * block_len, block_len)
        target = pl.multiple_of(index * block_len, block_len)
        outgoing[pl.ds(target, block_len)] = table[pl.ds(source, block_len)]
        return carry

    lax.fori_loop(0, asked.shape[0], one, 0)


def absorb_kernel(pieces, *refs):
    tokens, (query_weight, key_absorb, gain, out) = refs[:pieces], refs[pieces:]
    heads, width, _ = key_absorb.shape
    scale = gain[...].astype(f32)
    for piece in range(pieces):
        queries = jnp.dot(tokens[piece][...], query_weight[...], preferred_element_type=f32).astype(bf16)
        for head in range(heads):
            part = queries[:, head * width : (head + 1) * width]
            out[piece, head] = rms(
                jnp.dot(part, key_absorb[head], preferred_element_type=f32), scale
            ).astype(bf16)


def attend_kernel(
    groups, chosen, absorbed, table, arrived, value_absorb, head_gain, out_weight, *rest
):
    outs, (store, keys, mixed) = rest[: len(groups)], rest[len(groups) :]
    me, span = lax.axis_index("tp"), lax.axis_index("kv")
    block_count, picks = chosen.shape
    span_rows = table.shape[0]
    block_len = span_rows // block_count
    _, heads, rows, latent_width = absorbed.shape
    per_shard = rows // block_len
    store[pl.ds(0, span_rows)] = table[...]
    store[pl.ds(span_rows, arrived.shape[0])] = arrived[...]
    lanes = heads * block_len
    key_row = lax.broadcasted_iota(jnp.int32, (block_len, lanes), 0)
    query_row = lax.broadcasted_iota(jnp.int32, (block_len, lanes), 1) % block_len
    causal = key_row <= query_row
    scale = latent_width ** (-0.5)
    for slot, group in enumerate(groups):
        for inner in range(per_shard):
            turn = (slot * per_shard + inner) % 2
            local = jnp.bitwise_xor(me, group) * per_shard + inner
            block = span * block_count + local
            seen = []
            for pick in range(picks):
                target = chosen[local, pick]
                owner, within = target // block_count, target % block_count
                near = jnp.bitwise_xor(within // per_shard, me) * per_shard + within % per_shard
                source = jnp.where(owner == span, near, block_count + owner) * block_len
                keys[turn, pl.ds(pick * block_len, block_len)] = store[
                    pl.ds(pl.multiple_of(source, block_len), block_len)
                ]
                seen.append(target < block)
            query = absorbed[slot, :, pl.ds(inner * block_len, block_len), :].reshape(
                lanes, latent_width
            )
            near_keys = keys[turn]
            scores = lax.dot_general(
                near_keys, query, (((1,), (1,)), ((), ())), preferred_element_type=f32
            ) * scale
            parts = []
            for pick in range(picks):
                part = scores[pick * block_len : (pick + 1) * block_len]
                if pick == 0:
                    part = jnp.where(causal, part, -jnp.inf)
                else:
                    part = part + jnp.where(seen[pick], 0.0, -jnp.inf).astype(f32)
                parts.append(part)
            scores = jnp.concatenate(parts, axis=0)
            top = jnp.max(scores, axis=0, keepdims=True)
            raised = jnp.exp(scores - top)
            total = jnp.sum(raised, axis=0, keepdims=True)
            weights = (raised * (1.0 / total)).astype(bf16)
            out = lax.dot_general(
                weights, near_keys, (((0,), (0,)), ((), ())), preferred_element_type=f32
            ).astype(bf16)
            first = slot * rows + inner * block_len
            for head in range(heads):
                mixed[head, pl.ds(first, block_len)] = out[
                    head * block_len : (head + 1) * block_len
                ]
    parts = []
    for head in range(heads):
        values = jnp.dot(mixed[head], value_absorb[head], preferred_element_type=f32)
        parts.append(rms(values, head_gain[pl.ds(head, 1)].astype(f32)).astype(bf16))
    head_out = jnp.concatenate(parts, axis=1)
    for slot in range(len(groups)):
        outs[slot][...] = jnp.dot(
            head_out[slot * rows : (slot + 1) * rows],
            out_weight[...],
            preferred_element_type=f32,
        ).astype(bf16)


def body(
    tokens,
    query_weight,
    latent_weight,
    key_absorb,
    query_gain,
    latent_gain,
    value_absorb,
    head_gain,
    out_weight,
    chosen,
):
    shards = lax.axis_size("tp")
    spans = lax.axis_size("kv")
    rows, model = tokens.shape
    heads, width, latent_width = key_absorb.shape
    block_count, picks = chosen.shape
    per_shard = block_count // shards
    block_len = rows // per_shard
    shape = jax.ShapeDtypeStruct

    def swap(array, step):
        return lax.ppermute(array, "tp", [(i, i ^ step) for i in range(shards)])

    owner_of = chosen // block_count
    within = chosen % block_count
    matches = owner_of[:, :, None] == jnp.arange(spans, dtype=jnp.int32)[None, None, :]
    wanted = jnp.max(jnp.where(matches, within[:, :, None], 0), axis=(0, 1))

    own = call(
        latent_kernel,
        shape((rows, latent_width), bf16),
        [VMEM] * 3,
        flops=2 * rows * model * latent_width,
    )(tokens, latent_weight, latent_gain)
    core = swap(own, 1)
    far = swap(own, 2)
    diag = swap(own, 3)
    asked = lax.all_to_all(wanted, "kv", split_axis=0, concat_axis=0, tiled=True)
    tokens_far = swap(tokens, 2)
    tokens_core = swap(tokens, 1)
    tokens_diag = swap(tokens_far, 1)
    table, outgoing = call(
        functools.partial(pick_kernel, per_shard),
        [
            shape((block_count * block_len, latent_width), bf16),
            shape((spans * block_len, latent_width), bf16),
        ],
        [SMEM] + [VMEM] * 4,
    )(asked, own, core, far, diag)
    arrived = lax.all_to_all(
        outgoing.reshape(spans, block_len, latent_width),
        "kv",
        split_axis=0,
        concat_axis=0,
        tiled=True,
    ).reshape(spans * block_len, latent_width)

    def absorb(pieces):
        return call(
            functools.partial(absorb_kernel, len(pieces)),
            shape((len(pieces), heads, rows, latent_width), bf16),
            [VMEM] * (len(pieces) + 3),
            flops=2 * len(pieces) * rows * model * heads * width,
        )(*pieces, query_weight, key_absorb, query_gain)

    near_queries = absorb([tokens, tokens_core])
    far_queries = absorb([tokens_far, tokens_diag])

    def attend(groups, queries):
        return call(
            functools.partial(attend_kernel, groups),
            [shape((rows, model), bf16)] * len(groups),
            [SMEM] + [VMEM] * 6,
            scratch=[
                pltpu.VMEM(((block_count + spans) * block_len, latent_width), bf16),
                pltpu.VMEM((2, picks * block_len, latent_width), bf16),
                pltpu.VMEM((heads, len(groups) * rows, latent_width), bf16),
            ],
            flops=8 * len(groups) * per_shard * heads * block_len * picks * block_len * latent_width,
        )(chosen, queries, table, arrived, value_absorb, head_gain, out_weight)

    far_sum, far_send = attend((2, 3), far_queries)
    far_got = swap(far_send, 1)
    far_total = (far_sum.astype(f32) + far_got.astype(f32)).astype(bf16)
    far_in = swap(far_total, 2)
    near_sum, near_send = attend((0, 1), near_queries)
    near_got = swap(near_send, 1)
    return (near_sum.astype(f32) + near_got.astype(f32) + far_in.astype(f32)).astype(bf16)


def solution(mesh):
    return jax.shard_map(
        body,
        mesh=mesh,
        in_specs=(
            P(("kv", "tp"), None),
            P(None, "tp"),
            P(),
            P("tp", None, None),
            P(),
            P(),
            P("tp", None, None),
            P("tp", None),
            P("tp", None),
            P("kv", None),
        ),
        out_specs=P(("kv", "tp"), None),
        check_vma=False,
    )
```

time: 102 us -> 76.4 us (0.75)
  waiting for transfers between devices: 50.6 us -> 25.3 us
  Pallas kernels: 0 us -> 21.8 us
  between operations: 13.6 us -> 0.1 us
  blocking collectives: 0 us -> 12.6 us
  matrix products: 9.61 us -> 0 us
  other arithmetic: 10.6 us -> 2.11 us
  starting transfers between devices: 12.8 us -> 10.4 us
    reduce_scatter x1 -> x0, waiting for transfers between devices: 29.4 us -> none  [body(): lax.psum_scatter(jnp.dot(head_out, out_weight, preferred_element_type=jnp...]
    pallas_call x0 -> x6, Pallas kernels: none -> 21.8 us  [the longest x2 10.9 us: attend(): call(functools.partial(attend_kernel, groups), [shape((rows, model), bf16...]
    ppermute x0 -> x9, waiting for transfers between devices: none -> 21.1 us  [swap(): return lax.ppermute(array, 'tp', [(i, i ^ step) for i in range(shards)])]
    all_to_all x0 -> x1, blocking collectives: none -> 12.6 us  [body(): lax.all_to_all(wanted, 'kv', split_axis=0, concat_axis=0, tiled=True)]
    all_gather x1 -> x0, waiting for transfers between devices: 11.5 us -> none  [body(): shard_rows = lax.all_gather(tokens, 'tp', axis=0, tiled=True)]
    dot_general x7 -> x0, matrix products: 9.61 us -> none  [the longest x1 2.65 us: body(): jnp.dot(shard_rows, latent_weight, preferred_element_type=jnp.float32)]
    all_to_all x2 -> x1, starting transfers between devices: 12.8 us -> 3.41 us  [body(): lax.all_to_all(outgoing.reshape(spans, block_len, latent_width), 'kv', sp...]
    ppermute x0 -> x9, starting transfers between devices: none -> 7.01 us  [swap(): return lax.ppermute(array, 'tp', [(i, i ^ step) for i in range(shards)])]
  transfers between devices with their start and end apart: 4 -> 10, of which waited for: 4 -> 3; matrix products, arithmetic and copies ran while one was open for 8% -> 2% of each run, Pallas kernels for 0% -> 29%
where the time goes in v1:
time: 76.4 us; the launch traced here: 75.9 us
  waiting for transfers between devices  25.3 us (33%)
  Pallas kernels  21.8 us (29%)
  blocking collectives  12.6 us (16%)
  starting transfers between devices  10.4 us (14%)
  local copies, waits for them, and re-layouts  3.64 us (5%)
  other arithmetic  2.11 us (3%)
    ppermute x9, waiting for transfers between devices, swap(): return lax.ppermute(array, 'tp', [(i, i ^ step) for i in range(shards)])  21.1 us
    all_to_all x1, blocking collectives, body(): lax.all_to_all(wanted, 'kv', split_axis=0, concat_axis=0, tiled=True)  12.6 us
    pallas_call x2, Pallas kernels, attend(): call(functools.partial(attend_kernel, groups), [shape((rows, model), bf16...  10.9 us
    ppermute x9, starting transfers between devices, swap(): return lax.ppermute(array, 'tp', [(i, i ^ step) for i in range(shards)])  7.01 us
    pallas_call x2, Pallas kernels, absorb(): call(functools.partial(absorb_kernel, len(pieces)), shape((len(pieces), h...  6.71 us
    all_to_all x1, waiting for transfers between devices, body(): lax.all_to_all(outgoing.reshape(spans, block_len, latent_width), 'kv', sp...  4.19 us
    unnamed x22, local copies, waits for them, and re-layouts  3.56 us
    all_to_all x1, starting transfers between devices, body(): lax.all_to_all(outgoing.reshape(spans, block_len, latent_width), 'kv', sp...  3.41 us
  transfers between devices with their start and end apart: 10, of which 3 were waited for; matrix products, arithmetic and copies ran while one was open for 2% of the time, Pallas kernels for 29%

profile of v1, /device:TPU:0, one launch (start us, length us, event | category | flops | bytes accessed | tf_op | source)
XLA Modules:
  0.0 75.9 jit_solution(11549428937240154422)
XLA Ops:
  0.0 3.0 %collective-permute-start.5 = (bf16[128,2048]{1,0:T(8,128)(2,1)}, bf16[128,2048]{1,0:T(8,128)(2,1)S(1)}, u32[]{:S(2)}, u32[]{:S(2)}) collective-permute-start(bf16[128,2048]{1,0:T(8,128)(2,1)} %tokens.1), channel_id=1, source_target_pairs={{0,2},{1,3},{2,0},{3,1},{4,6},{5,7},{6,4},{7,5},{8,10},{9,11},{10,... | collective-permute-start | bytes 1572872 | tf_op jit(solution)/shard_map/ppermute | solution.py:167
  3.0 2.4 %shard_map.101.own = bf16[128,256]{1,0:T(8,128)(2,1)} custom-call(bf16[128,2048]{1,0:T(8,128)(2,1)} %tokens.1, bf16[2048,256]{1,0:T(8,128)(2,1)} %weight.1, bf16[256]{0:T(256)(128)(2,1)} %gain.1), custom_call_target="tpu_custom_call" | custom-call | flops 134217728 | tf_op jit(solution)/shard_map/pallas_call | solution.py:174
  5.4 1.8 %collective-permute-start.3 = (bf16[128,256]{1,0:T(8,128)(2,1)}, bf16[128,256]{1,0:T(8,128)(2,1)S(1)}, u32[]{:S(2)}, u32[]{:S(2)}) collective-permute-start(bf16[128,256]{1,0:T(8,128)(2,1)} %shard_map.101.own), channel_id=1, source_target_pairs={{0,3},{1,2},{2,1},{3,0},{4,7},{5,6},{6,5},{7,4},{8,11},{9,10},{10,... | collective-permute-start | bytes 196616 | tf_op jit(solution)/shard_map/ppermute | solution.py:167
  7.2 8.7 %collective-permute-done.5.refs_0_ = bf16[128,2048]{1,0:T(8,128)(2,1)S(1)} collective-permute-done((bf16[128,2048]{1,0:T(8,128)(2,1)}, bf16[128,2048]{1,0:T(8,128)(2,1)S(1)}, u32[]{:S(2)}, u32[]{:S(2)}) %collective-permute-start.5) | collective-permute-done | bytes 524320 | tf_op jit(solution)/shard_map/ppermute | solution.py:167
  16.0 0.1 select_reduce_fusion
  16.2 12.6 %all_to_all.16 = s32[8,1,1]{2,1,0:T(1,128)S(1)} all-to-all(s32[8,1,1]{2,1,0:T(1,128)S(1)} %copy.13), channel_id=1, replica_groups=mesh['kv'=8,'tp'=4] {'kv'}, dimensions={0} | all-to-all | bytes 64 | tf_op jit(solution)/shard_map/all_to_all | solution.py:183
  28.8 0.8 %reduce.asked = s32[8]{0:T(128)} reduce(s32[8,1,1]{2,1,0:T(1,128)S(1)} %all_to_all.16, s32[]{:T(128)} %constant.25.clone.1), dimensions={1,2}, to_apply=%all_to_all.11.reduce_sub_computation | reduce | bytes 68 | tf_op jit(solution)/shard_map/all_to_all | solution.py:183
  29.6 0.6 copy-done.7
  30.2 0.6 copy-done.9
  30.9 1.9 %shard_map.102 = (bf16[512,256]{1,0:T(8,128)(2,1)}, bf16[512,256]{1,0:T(8,128)(2,1)}) custom-call(s32[8]{0:T(128)} %reduce.asked, bf16[128,256]{1,0:T(8,128)(2,1)} %shard_map.101.own, bf16[128,256]{1,0:T(8,128)(2,1)} %copy-done.7, bf16[128,256]{1,0:T(8,128)(2,1)} %copy-done.8, bf16[128,256]{1,0:T(8,128)(2,1)} %copy-done.9), custom_call_target="tpu_custom_call" | custom-call | tf_op jit(solution)/shard_map/pallas_call | solution.py:187
  32.7 3.4 %all-to-all-start.1 = ((bf16[8,64,256]{2,1,0:T(8,128)(2,1)}), bf16[8,64,256]{2,1,0:T(8,128)(2,1)S(1)}, u32[]{:S(2)}, u32[]{:S(2)}) async-start(bf16[8,64,256]{2,1,0:T(8,128)(2,1)} %bitcast.5), calls=%async_computation.1 | async-start | bytes 524288 | tf_op jit(solution)/shard_map/all_to_all | solution.py:195
  36.3 0.8 %copy-done.3 = bf16[128,2048]{1,0:T(8,128)(2,1)} copy-done((bf16[128,2048]{1,0:T(8,128)(2,1)}, bf16[128,2048]{1,0:T(8,128)(2,1)S(1)}, u32[]{:S(2)}) %copy-start.3) | copy-done | bytes 524312
  37.1 3.4 %shard_map.104.absorbed = bf16[2,2,128,256]{3,2,1,0:T(8,128)(2,1)} custom-call(bf16[128,2048]{1,0:T(8,128)(2,1)} %copy-done.2, bf16[128,2048]{1,0:T(8,128)(2,1)} %copy-done.3, bf16[2048,256]{1,0:T(8,128)(2,1)} %refs_2_.3, bf16[2,128,256]{2,1,0:T(8,128)(2,1)} %refs_3_.3, bf16[256]{0:T(256)(128)(2,1)} %refs_4_.3), custom_call_target="tpu_custom_call" | custom-call | flops 268435456 | tf_op jit(solution)/shard_map/pallas_call | solution.py:204
  40.4 4.2 %all-to-all-done.1 = bf16[8,64,256]{2,1,0:T(8,128)(2,1)S(1)} async-done(((bf16[8,64,256]{2,1,0:T(8,128)(2,1)}), bf16[8,64,256]{2,1,0:T(8,128)(2,1)S(1)}, u32[]{:S(2)}, u32[]{:S(2)}) %all-to-all-start.1) | async-done | bytes 262176 | tf_op jit(solution)/shard_map/all_to_all | solution.py:195
  44.6 0.7 copy-done.6
  45.3 5.4 %shard_map.105 = (bf16[128,2048]{1,0:T(8,128)(2,1)}, bf16[128,2048]{1,0:T(8,128)(2,1)}) custom-call(s32[8,11]{1,0:T(8,128)} %chosen.3, bf16[2,2,128,256]{3,2,1,0:T(8,128)(2,1)} %shard_map.104.absorbed, bf16[512,256]{1,0:T(8,128)(2,1)} %get-tuple-element.11.table, bf16[512,256]{1,0:T(8,128)(2,1)} %bitcast.3, bf16[2,256,128]{2,1,0:T(8,128)(2,1)} %value_absorb.3, ...), custom_call_target="tpu_custom_call" | custom-call | flops 738197504 | tf_op jit(solution)/shard_map/pallas_call | solution.py:215
  50.7 0.8 %copy-done.5 = bf16[128,2048]{1,0:T(8,128)(2,1)} copy-done((bf16[128,2048]{1,0:T(8,128)(2,1)}, bf16[128,2048]{1,0:T(8,128)(2,1)S(1)}, u32[]{:S(2)}) %copy-start.5) | copy-done | bytes 524312
  51.5 3.4 %shard_map.100.absorbed = bf16[2,2,128,256]{3,2,1,0:T(8,128)(2,1)} custom-call(bf16[128,2048]{1,0:T(8,128)(2,1)} %tokens.1, bf16[128,2048]{1,0:T(8,128)(2,1)} %copy-done.5, bf16[2048,256]{1,0:T(8,128)(2,1)} %refs_2_.3, bf16[2,128,256]{2,1,0:T(8,128)(2,1)} %refs_3_.3, bf16[256]{0:T(256)(128)(2,1)} %refs_4_.3), custom_call_target="tpu_custom_call" | custom-call | flops 268435456 | tf_op jit(solution)/shard_map/pallas_call | solution.py:204
  54.9 5.5 %shard_map.103 = (bf16[128,2048]{1,0:T(8,128)(2,1)}, bf16[128,2048]{1,0:T(8,128)(2,1)}) custom-call(s32[8,11]{1,0:T(8,128)} %chosen.3, bf16[2,2,128,256]{3,2,1,0:T(8,128)(2,1)} %shard_map.100.absorbed, bf16[512,256]{1,0:T(8,128)(2,1)} %get-tuple-element.11.table, bf16[512,256]{1,0:T(8,128)(2,1)} %bitcast.4, bf16[2,256,128]{2,1,0:T(8,128)(2,1)} %value_absorb.3, ...), custom_call_target="tpu_custom_call" | custom-call | flops 738197504 | tf_op jit(solution)/shard_map/pallas_call | solution.py:215
  60.3 0.5 collective-permute-start.4
  60.9 0.1 add_convert_fusion.1
  61.0 1.6 %collective-permute-start.8 = (bf16[128,2048]{1,0:T(8,128)(2,1)S(1)}, bf16[128,2048]{1,0:T(8,128)(2,1)S(1)}, u32[]{:S(2)}, u32[]{:S(2)}) collective-permute-start(bf16[128,2048]{1,0:T(8,128)(2,1)S(1)} %add_convert_fusion.1), channel_id=1, source_target_pairs={{0,2},{1,3},{2,0},{3,1},{4,6},{5,7},{6,4},{7,5},{8,10},{9,11},{10,... | collective-permute-start | bytes 1572872 | tf_op jit(solution)/shard_map/ppermute | solution.py:167
  62.6 12.3 %collective-permute-done.8 = bf16[128,2048]{1,0:T(8,128)(2,1)S(1)} collective-permute-done((bf16[128,2048]{1,0:T(8,128)(2,1)S(1)}, bf16[128,2048]{1,0:T(8,128)(2,1)S(1)}, u32[]{:S(2)}, u32[]{:S(2)}) %collective-permute-start.8) | collective-permute-done | bytes 524320 | tf_op jit(solution)/shard_map/ppermute | solution.py:167
  74.9 1.0 %add_convert_fusion = bf16[128,2048]{1,0:T(8,128)(2,1)} fusion(bf16[128,2048]{1,0:T(8,128)(2,1)S(1)} %collective-permute-done.8, bf16[128,2048]{1,0:T(8,128)(2,1)S(1)} %collective-permute-done.4, bf16[128,2048]{1,0:T(8,128)(2,1)S(1)} %copy-done.4), kind=kLoop, calls=%fused_computation | loop fusion | flops 1572864 | bytes 2097152 | tf_op jit(solution)/shard_map/convert_element_type | solution.py:233
  (31 shorter events, 0.3 us)
Async XLA Ops:
  0.0 7.2 %copy-start.10 = (s32[8,11]{1,0:T(8,128)S(1)}, s32[8,11]{1,0:T(8,128)}, u32[]{:S(2)}) copy-start(s32[8,11]{1,0:T(8,128)} %chosen.3) | copy-start | bytes 1060
  0.0 16.0 %collective-permute-start.5 = (bf16[128,2048]{1,0:T(8,128)(2,1)}, bf16[128,2048]{1,0:T(8,128)(2,1)S(1)}, u32[]{:S(2)}, u32[]{:S(2)}) collective-permute-start(bf16[128,2048]{1,0:T(8,128)(2,1)} %tokens.1), channel_id=1, source_target_pairs={{0,2},{1,3},{2,0},{3,1},{4,6},{5,7},{6,4},{7,5},{8,10},{9,11},{10,... | collective-permute-start | bytes 1572872 | tf_op jit(solution)/shard_map/ppermute | solution.py:167
  5.4 30.8 %copy-start = (bf16[128,2048]{1,0:T(8,128)(2,1)S(1)}, bf16[128,2048]{1,0:T(8,128)(2,1)}, u32[]{:S(2)}) copy-start(bf16[128,2048]{1,0:T(8,128)(2,1)} %tokens.1) | copy-start | bytes 1572868
  5.4 24.2 %collective-permute-start.1 = (bf16[128,256]{1,0:T(8,128)(2,1)}, bf16[128,256]{1,0:T(8,128)(2,1)S(1)}, u32[]{:S(2)}, u32[]{:S(2)}) collective-permute-start(bf16[128,256]{1,0:T(8,128)(2,1)} %shard_map.101.own), channel_id=1, source_target_pairs={{0,1},{1,0},{2,3},{3,2},{4,5},{5,4},{6,7},{7,6},{8,9},{9,8},{10,11... | collective-permute-start | bytes 196616 | tf_op jit(solution)/shard_map/ppermute | solution.py:167
  5.4 24.2 %collective-permute-start.2 = (bf16[128,256]{1,0:T(8,128)(2,1)}, bf16[128,256]{1,0:T(8,128)(2,1)S(1)}, u32[]{:S(2)}, u32[]{:S(2)}) collective-permute-start(bf16[128,256]{1,0:T(8,128)(2,1)} %shard_map.101.own), channel_id=1, source_target_pairs={{0,2},{1,3},{2,0},{3,1},{4,6},{5,7},{6,4},{7,5},{8,10},{9,11},{10,... | collective-permute-start | bytes 196616 | tf_op jit(solution)/shard_map/ppermute | solution.py:167
  5.4 24.2 %collective-permute-start.3 = (bf16[128,256]{1,0:T(8,128)(2,1)}, bf16[128,256]{1,0:T(8,128)(2,1)S(1)}, u32[]{:S(2)}, u32[]{:S(2)}) collective-permute-start(bf16[128,256]{1,0:T(8,128)(2,1)} %shard_map.101.own), channel_id=1, source_target_pairs={{0,3},{1,2},{2,1},{3,0},{4,7},{5,6},{6,5},{7,4},{8,11},{9,10},{10,... | collective-permute-start | bytes 196616 | tf_op jit(solution)/shard_map/ppermute | solution.py:167
  16.0 20.3 %copy-start.2 = (bf16[128,2048]{1,0:T(8,128)(2,1)}, bf16[128,2048]{1,0:T(8,128)(2,1)S(1)}, u32[]{:S(2)}) copy-start(bf16[128,2048]{1,0:T(8,128)(2,1)S(1)} %collective-permute-done.5.refs_0_) | copy-start | bytes 1572868
  16.0 20.3 %collective-permute-start.6 = (bf16[128,2048]{1,0:T(8,128)(2,1)S(1)}, bf16[128,2048]{1,0:T(8,128)(2,1)S(1)}, u32[]{:S(2)}, u32[]{:S(2)}) collective-permute-start(bf16[128,2048]{1,0:T(8,128)(2,1)S(1)} %collective-permute-done.5.refs_0_), channel_id=1, source_target_pairs={{0,1},{1,0},{2,3},{3,2},{4,5},{5,4},{6,7},{7,6},{8,9},{9,8},{10,11... | collective-permute-start | bytes 1572872 | tf_op jit(solution)/shard_map/ppermute | solution.py:167
  29.6 0.6 copy-start.7
  29.6 0.6 copy-start.8
  30.2 0.6 copy-start.9
  32.7 11.9 %all-to-all-start.1 = ((bf16[8,64,256]{2,1,0:T(8,128)(2,1)}), bf16[8,64,256]{2,1,0:T(8,128)(2,1)S(1)}, u32[]{:S(2)}, u32[]{:S(2)}) async-start(bf16[8,64,256]{2,1,0:T(8,128)(2,1)} %bitcast.5), calls=%async_computation.1 | async-start | bytes 524288 | tf_op jit(solution)/shard_map/all_to_all | solution.py:195
  36.2 14.5 %collective-permute-start = (bf16[128,2048]{1,0:T(8,128)(2,1)S(1)}, bf16[128,2048]{1,0:T(8,128)(2,1)S(1)}, u32[]{:S(2)}, u32[]{:S(2)}) collective-permute-start(bf16[128,2048]{1,0:T(8,128)(2,1)S(1)} %copy-done), channel_id=1, source_target_pairs={{0,1},{1,0},{2,3},{3,2},{4,5},{5,4},{6,7},{7,6},{8,9},{9,8},{10,11... | collective-permute-start | bytes 1572872 | tf_op jit(solution)/shard_map/ppermute | solution.py:167
  36.3 0.8 %copy-start.3 = (bf16[128,2048]{1,0:T(8,128)(2,1)}, bf16[128,2048]{1,0:T(8,128)(2,1)S(1)}, u32[]{:S(2)}) copy-start(bf16[128,2048]{1,0:T(8,128)(2,1)S(1)} %collective-permute-done.6.refs_1_) | copy-start | bytes 1572868
  44.6 0.7 copy-start.6
  50.7 10.1 %collective-permute-start.7 = (bf16[128,2048]{1,0:T(8,128)(2,1)}, bf16[128,2048]{1,0:T(8,128)(2,1)S(1)}, u32[]{:S(2)}, u32[]{:S(2)}) collective-permute-start(bf16[128,2048]{1,0:T(8,128)(2,1)} %get-tuple-element.16), channel_id=1, source_target_pairs={{0,1},{1,0},{2,3},{3,2},{4,5},{5,4},{6,7},{7,6},{8,9},{9,8},{10,11... | collective-permute-start | bytes 1572872 | tf_op jit(solution)/shard_map/ppermute | solution.py:167
  50.7 0.8 %copy-start.5 = (bf16[128,2048]{1,0:T(8,128)(2,1)}, bf16[128,2048]{1,0:T(8,128)(2,1)S(1)}, u32[]{:S(2)}) copy-start(bf16[128,2048]{1,0:T(8,128)(2,1)S(1)} %collective-permute-done.refs_1_) | copy-start | bytes 1572868
  54.9 6.0 %copy-start.1 = (bf16[128,2048]{1,0:T(8,128)(2,1)S(1)}, bf16[128,2048]{1,0:T(8,128)(2,1)}, u32[]{:S(2)}) copy-start(bf16[128,2048]{1,0:T(8,128)(2,1)} %get-tuple-element.15) | copy-start | bytes 1572868
  60.3 2.2 %collective-permute-start.4 = (bf16[128,2048]{1,0:T(8,128)(2,1)}, bf16[128,2048]{1,0:T(8,128)(2,1)S(1)}, u32[]{:S(2)}, u32[]{:S(2)}) collective-permute-start(bf16[128,2048]{1,0:T(8,128)(2,1)} %get-tuple-element.14), channel_id=1, source_target_pairs={{0,1},{1,0},{2,3},{3,2},{4,5},{5,4},{6,7},{7,6},{8,9},{9,8},{10,11... | collective-permute-start | bytes 1572872 | tf_op jit(solution)/shard_map/ppermute | solution.py:167
  60.8 14.1 %copy-start.4 = (bf16[128,2048]{1,0:T(8,128)(2,1)S(1)}, bf16[128,2048]{1,0:T(8,128)(2,1)}, u32[]{:S(2)}) copy-start(bf16[128,2048]{1,0:T(8,128)(2,1)} %get-tuple-element.13) | copy-start | bytes 1572868
  61.0 13.9 %collective-permute-start.8 = (bf16[128,2048]{1,0:T(8,128)(2,1)S(1)}, bf16[128,2048]{1,0:T(8,128)(2,1)S(1)}, u32[]{:S(2)}, u32[]{:S(2)}) collective-permute-start(bf16[128,2048]{1,0:T(8,128)(2,1)S(1)} %add_convert_fusion.1), channel_id=1, source_target_pairs={{0,2},{1,3},{2,0},{3,1},{4,6},{5,7},{6,4},{7,5},{8,10},{9,11},{10,... | collective-permute-start | bytes 1572872 | tf_op jit(solution)/shard_map/ppermute | solution.py:167

commit v2 on v1

v2 whole, which is shorter than its diff:
```python
import functools
import math

import jax
import jax.numpy as jnp
from jax import lax
from jax.experimental import pallas as pl
from jax.experimental.pallas import tpu as pltpu
from jax.sharding import PartitionSpec as P


epsilon = 1e-06
f32 = jnp.float32
bf16 = jnp.bfloat16
VMEM = pl.BlockSpec(memory_space=pltpu.VMEM)
SLACK = 2
LANES = 128
ABSORB = 8 << 20
FAR = 54 << 20
NEAR = 46 << 20
HBM = pl.BlockSpec(memory_space=pl.ANY)
SMEM = pl.BlockSpec(memory_space=pltpu.SMEM)


def split(value, count):
    if count & (count - 1) == 0:
        return value >> (count.bit_length() - 1), value & (count - 1)
    return value // count, value % count


def near_slot(within, me, per_shard):
    if per_shard & (per_shard - 1) == 0:
        return within ^ (me * per_shard)
    shard, inner = split(within, per_shard)
    return (shard ^ me) * per_shard + inner


def rms(values, gain):
    return values * lax.rsqrt(jnp.mean(values * values, axis=-1, keepdims=True) + epsilon) * gain


def call(kernel, out_shape, in_specs, scratch=(), flops=0, grant=None):
    many = isinstance(out_shape, (list, tuple))

    def run(*arrays):
        held = [array for array, spec in zip(arrays, in_specs) if spec is VMEM]
        held += list(out_shape) if many else [out_shape]
        held += [array for array in scratch if hasattr(array, "shape")]
        size = sum(math.prod(array.shape) * 2 for array in held)
        return pl.pallas_call(
            kernel,
            out_shape=out_shape,
            in_specs=in_specs,
            out_specs=[VMEM] * len(out_shape) if many else VMEM,
            scratch_shapes=list(scratch),
            compiler_params=pltpu.CompilerParams(vmem_limit_bytes=grant or size + (SLACK << 20)),
            cost_estimate=pl.CostEstimate(flops=flops, bytes_accessed=size, transcendentals=0),
        )(*arrays)

    return run


def pick_kernel(per_shard, asked, own, core, far, diag, outgoing, table):
    me = lax.axis_index("tp")
    rows = own.shape[0]
    block_len = rows // per_shard
    for index, part in enumerate((own, core, far, diag)):
        table[pl.ds(index * rows, rows)] = part[...]

    def one(index, carry):
        within = asked[index, 0, 0]
        slot = near_slot(within, me, per_shard)
        source = pl.multiple_of(slot * block_len, block_len)
        target = pl.multiple_of(index * block_len, block_len)
        outgoing[pl.ds(target, block_len)] = table[pl.ds(source, block_len)]
        return carry

    lax.fori_loop(0, asked.shape[0], one, 0)


def absorb_kernel(pieces, *refs):
    tokens, (query_weight, key_absorb, gain, out) = refs[:pieces], refs[pieces:]
    heads, width, _ = key_absorb.shape
    scale = gain[...].astype(f32)
    products = [
        jnp.dot(part[...], query_weight[...], preferred_element_type=f32) for part in tokens
    ]
    for piece in range(pieces):
        queries = products[piece].astype(bf16)
        for head in range(heads):
            part = queries[:, head * width : (head + 1) * width]
            out[piece, head] = rms(
                jnp.dot(part, key_absorb[head], preferred_element_type=f32), scale
            ).astype(bf16)


def attend_kernel(
    groups, chosen, absorbed, own, core, far, diag, arrived, value_absorb, head_gain, *rest
):
    out, store, keys, mixed = rest[-4:]
    me, span = lax.axis_index("tp"), lax.axis_index("kv")
    block_count, picks = chosen.shape
    _, heads, rows, latent_width = absorbed.shape
    span_rows = 4 * rows
    block_len = span_rows // block_count
    per_shard = rows // block_len
    width = keys.shape[1]
    for index, part in enumerate((own, core, far, diag)):
        store[pl.ds(index * rows, rows)] = part[...]
    store[pl.ds(span_rows, arrived.shape[0])] = arrived[...]
    lanes = heads * block_len
    query_row = lax.broadcasted_iota(jnp.int32, (lanes, LANES), 0) % block_len
    lane = lax.broadcasted_iota(jnp.int32, (lanes, LANES), 1)
    causal = lane <= query_row
    pick_of_lane = lax.broadcasted_iota(jnp.int32, (1, LANES), 1) // block_len
    per_tile = LANES // block_len
    scale = latent_width ** (-0.5) * math.log2(math.e)

    def gather(turn):
        slot, inner = turn // per_shard, turn % per_shard
        local = jnp.bitwise_xor(me, groups[slot]) * per_shard + inner
        block = span * block_count + local
        if width > picks * block_len:
            rest = width - picks * block_len
            keys[turn, pl.ds(picks * block_len, rest)] = jnp.zeros((rest, latent_width), bf16)
        biases = []
        for pick in range(picks):
            target = chosen[local, pick]
            owner, within = split(target, block_count)
            near = near_slot(within, me, per_shard)
            source = jnp.where(owner == span, near, block_count + owner) * block_len
            keys[turn, pl.ds(pick * block_len, block_len)] = store[
                pl.ds(pl.multiple_of(source, block_len), block_len)
            ]
            biases.append(jnp.where((target < block) | (pick == 0), 0.0, -jnp.inf).astype(f32))
        query = absorbed[groups[slot], :, pl.ds(inner * block_len, block_len), :].reshape(
            lanes, latent_width
        )
        scores = lax.dot_general(
            query, keys[turn], (((1,), (1,)), ((), ())), preferred_element_type=f32
        )
        return scores, biases

    def weigh(scores, biases):
        parts = []
        for tile in range(width // LANES):
            part = scores[:, tile * LANES : (tile + 1) * LANES]
            bias = jnp.full((1, LANES), -jnp.inf, f32)
            for inside in range(per_tile):
                pick = tile * per_tile + inside
                if pick < picks:
                    bias = jnp.where(pick_of_lane == inside, biases[pick], bias)
            part = part + bias
            if tile == 0:
                part = jnp.where(causal | (lane >= block_len), part, -jnp.inf)
            parts.append(part)
        top = parts[0]
        for part in parts[1:]:
            top = jnp.maximum(top, part)
        top = jnp.max(top, axis=1, keepdims=True)
        raised = [jnp.exp2((part - top) * scale) for part in parts]
        total = raised[0]
        for part in raised[1:]:
            total = total + part
        share = 1.0 / jnp.sum(total, axis=1, keepdims=True)
        return jnp.concatenate([(part * share).astype(bf16) for part in raised], axis=1)

    def mix(turn, weights):
        out = jnp.dot(weights, keys[turn], preferred_element_type=f32).astype(bf16)
        for head in range(heads):
            mixed[head, pl.ds(turn * block_len, block_len)] = out[
                head * block_len : (head + 1) * block_len
            ]

    turns = len(groups) * per_shard
    ahead = gather(0)
    for turn in range(turns):
        current = ahead
        if turn + 1 < turns:
            ahead = gather(turn + 1)
        mix(turn, weigh(*current))
    parts = []
    for head in range(heads):
        values = jnp.dot(mixed[head], value_absorb[head], preferred_element_type=f32)
        parts.append(rms(values, head_gain[pl.ds(head, 1)].astype(f32)).astype(bf16))
    head_out = jnp.concatenate(parts, axis=1)
    for weight in rest[:-4]:
        head_out = jnp.dot(head_out, weight[...], preferred_element_type=f32).astype(bf16)
    out[...] = head_out


def project_kernel(half, near, far, first, second, third, fourth, out):
    span = lax.axis_index("kv")
    parity = jnp.bitwise_and(jnp.bitwise_xor(span, span >> 1), 1)
    rows = out.shape[0]
    depth = 2 * first.shape[0]
    here = pl.ds(half * rows, rows)
    direct = jnp.concatenate([first[...], second[...]], axis=0)
    relayed = jnp.concatenate([third[...], fourth[...]], axis=0)
    at = pl.multiple_of(parity * depth, depth)
    other = pl.multiple_of((1 - parity) * depth, depth)
    partial = jnp.dot(far[here, pl.ds(at, depth)], direct, preferred_element_type=f32)
    partial += jnp.dot(far[here, pl.ds(other, depth)], relayed, preferred_element_type=f32)
    total = near[here].astype(f32) + partial.astype(bf16).astype(f32)
    out[...] = total.astype(out.dtype)


def body(
    tokens,
    query_weight,
    latent_weight,
    key_absorb,
    query_gain,
    latent_gain,
    value_absorb,
    head_gain,
    out_weight,
    chosen,
):
    shards = lax.axis_size("tp")
    spans = lax.axis_size("kv")
    rows, model = tokens.shape
    heads, width, latent_width = key_absorb.shape
    block_count, picks = chosen.shape
    per_shard = block_count // shards
    block_len = rows // per_shard
    padded = -(-picks * block_len // LANES) * LANES
    shape = jax.ShapeDtypeStruct

    def swap(array, step):
        return lax.ppermute(array, "tp", [(i, i ^ step) for i in range(shards)])

    owner_of = chosen // block_count
    within = chosen % block_count
    matches = owner_of[:, :, None] == jnp.arange(spans, dtype=jnp.int32)[None, None, :]
    wanted = jnp.max(jnp.where(matches, within[:, :, None], 0), axis=(0, 1))
    wanted = jnp.broadcast_to(wanted[:, None, None], (spans, 1, LANES))

    own = rms(
        jnp.dot(tokens, latent_weight, preferred_element_type=f32), latent_gain.astype(f32)
    ).astype(bf16)
    core = swap(own, 1)
    far = swap(own, 2)
    diag = swap(own, 3)
    asked = lax.all_to_all(wanted, "kv", split_axis=0, concat_axis=0, tiled=True)
    tokens_far = swap(tokens, 2)
    tokens_core = swap(tokens, 1)
    tokens_diag = swap(tokens_far, 1)
    parity = jnp.bitwise_and(lax.axis_index("kv") ^ (lax.axis_index("kv") >> 1), 1)
    quarter = out_weight.shape[0] // 4
    piece_a = lax.dynamic_slice(out_weight, (2 * quarter * parity, 0), (quarter, model))
    piece_b = lax.dynamic_slice(out_weight, (2 * quarter * parity + quarter, 0), (quarter, model))

    def relay(array, step):
        return lax.ppermute(array, "kv", [(i, i ^ step) for i in range(spans)])

    far_weights = [swap(piece_a, 2), swap(piece_b, 2)]
    far_weights.append(relay(far_weights[0], 1))
    far_weights.append(relay(far_weights[1], 2))
    outgoing = call(
        functools.partial(pick_kernel, per_shard),
        shape((spans * block_len, latent_width), bf16),
        [SMEM] + [VMEM] * 4,
        scratch=[pltpu.VMEM((block_count * block_len, latent_width), bf16)],
    )(asked, own, core, far, diag)
    arrived = lax.all_to_all(
        outgoing.reshape(spans, block_len, latent_width),
        "kv",
        split_axis=0,
        concat_axis=0,
        tiled=True,
    ).reshape(spans * block_len, latent_width)

    def absorb(pieces):
        return call(
            functools.partial(absorb_kernel, len(pieces)),
            shape((len(pieces), heads, rows, latent_width), bf16),
            [VMEM] * (len(pieces) + 3),
            flops=2 * len(pieces) * rows * model * heads * width,
            grant=ABSORB,
        )(*pieces, query_weight, key_absorb, query_gain)

    queries = absorb([tokens, tokens_core, tokens_far, tokens_diag])

    def attend(groups, grant=None, weight=()):
        return call(
            functools.partial(attend_kernel, groups),
            shape((len(groups) * rows, model if weight else heads * width), bf16),
            [SMEM] + [VMEM] * (8 + len(weight)),
            scratch=[
                pltpu.VMEM(((block_count + spans) * block_len, latent_width), bf16),
                pltpu.VMEM((len(groups) * per_shard, padded, latent_width), bf16),
                pltpu.VMEM((heads, len(groups) * rows, latent_width), bf16),
            ],
            flops=8 * len(groups) * per_shard * heads * block_len * picks * block_len * latent_width,
            grant=grant,
        )(chosen, queries, own, core, far, diag, arrived, value_absorb, head_gain, *weight)

    far_heads = attend((2, 3), FAR)
    far_heads = swap(far_heads, 2)
    near_part = attend((0, 1), NEAR, (out_weight,))

    def project(half, dtype):
        return call(
            functools.partial(project_kernel, half),
            shape((rows, model), dtype),
            [VMEM] * 6,
            flops=2 * rows * heads * width * model,
        )(near_part, far_heads, *far_weights)

    core_part = project(1, bf16)
    core_part = swap(core_part, 1)
    own_part = project(0, f32)
    return (own_part + core_part.astype(f32)).astype(bf16)


def solution(mesh):
    return jax.shard_map(
        body,
        mesh=mesh,
        in_specs=(
            P(("kv", "tp"), None),
            P(None, "tp"),
            P(),
            P("tp", None, None),
            P(),
            P(),
            P("tp", None, None),
            P("tp", None),
            P("tp", None),
            P("kv", None),
        ),
        out_specs=P(("kv", "tp"), None),
        check_vma=False,
    )
```

time: 76.4 us -> 66.7 us (0.87)
  blocking collectives: 12.6 us -> 0 us
  starting transfers between devices: 10.4 us -> 22.5 us
  Pallas kernels: 21.8 us -> 13.1 us
  local copies, waits for them, and re-layouts: 3.64 us -> 1.6 us
  matrix products: 0 us -> 1.46 us
  other arithmetic: 2.11 us -> 1.13 us
  waiting for transfers between devices: 25.3 us -> 26.1 us
    all_to_all x1 -> x0, blocking collectives: 12.6 us -> none  [body(): lax.all_to_all(wanted, 'kv', split_axis=0, concat_axis=0, tiled=True)]
    pallas_call x6, Pallas kernels: 21.8 us -> 13.1 us  [run(): pl.pallas_call(kernel, out_shape=out_shape, in_specs=in_specs, out_specs=...]
    all_to_all x0 -> x1, waiting for transfers between devices: none -> 6.42 us  [body(): lax.all_to_all(wanted, 'kv', split_axis=0, concat_axis=0, tiled=True)]
    all_to_all x0 -> x1, starting transfers between devices: none -> 6.28 us  [body(): lax.all_to_all(wanted, 'kv', split_axis=0, concat_axis=0, tiled=True)]
    all_to_all x1, waiting for transfers between devices: 4.19 us -> 0.01 us  [body(): lax.all_to_all(outgoing.reshape(spans, block_len, latent_width), 'kv', sp...]
    ppermute x0 -> x2, starting transfers between devices: none -> 3.47 us  [relay(): return lax.ppermute(array, 'kv', [(i, i ^ step) for i in range(spans)])]
    unnamed x22 -> x42, local copies, waits for them, and re-layouts: 3.56 us -> 0.88 us
    ppermute x9 -> x10, starting transfers between devices: 7.01 us -> 8.62 us  [swap(): return lax.ppermute(array, 'tp', [(i, i ^ step) for i in range(shards)])]
  transfers between devices with their start and end apart: 10 -> 14, of which waited for: 3 -> 6; matrix products, arithmetic and copies ran while one was open for 2% -> 4% of each run, Pallas kernels for 29% -> 18%
where the time goes in v2:
time: 66.7 us; the launch traced here: 66.2 us
  waiting for transfers between devices  26.1 us (39%)
  starting transfers between devices  22.5 us (34%)
  Pallas kernels  13.1 us (20%)
  local copies, waits for them, and re-layouts  1.6 us (2%)
  matrix products  1.46 us (2%)
  other arithmetic  1.13 us (2%)
    ppermute x10, waiting for transfers between devices, swap(): return lax.ppermute(array, 'tp', [(i, i ^ step) for i in range(shards)])  19.7 us
    pallas_call x6, Pallas kernels, run(): pl.pallas_call(kernel, out_shape=out_shape, in_specs=in_specs, out_specs=...  13.1 us
    ppermute x10, starting transfers between devices, swap(): return lax.ppermute(array, 'tp', [(i, i ^ step) for i in range(shards)])  8.62 us
    all_to_all x1, waiting for transfers between devices, body(): lax.all_to_all(wanted, 'kv', split_axis=0, concat_axis=0, tiled=True)  6.42 us
    all_to_all x1, starting transfers between devices, body(): lax.all_to_all(wanted, 'kv', split_axis=0, concat_axis=0, tiled=True)  6.28 us
    all_to_all x1, starting transfers between devices, body(): lax.all_to_all(outgoing.reshape(spans, block_len, latent_width), 'kv', sp...  4.19 us
    ppermute x2, starting transfers between devices, relay(): return lax.ppermute(array, 'kv', [(i, i ^ step) for i in range(spans)])  3.47 us
    dot_general x1, matrix products, body(): jnp.dot(tokens, latent_weight, preferred_element_type=f32)  1.46 us
  transfers between devices with their start and end apart: 14, of which 6 were waited for; matrix products, arithmetic and copies ran while one was open for 4% of the time, Pallas kernels for 18%

profile of v2, /device:TPU:0, one launch (start us, length us, event | category | flops | bytes accessed | tf_op | source)
XLA Modules:
  0.0 66.2 jit_solution(11743127313214187476)
XLA Ops:
  0.0 3.0 %collective-permute-start.1 = (bf16[128,2048]{1,0:T(8,128)(2,1)}, bf16[128,2048]{1,0:T(8,128)(2,1)}, u32[]{:S(2)}, u32[]{:S(2)}) collective-permute-start(bf16[128,2048]{1,0:T(8,128)(2,1)} %refs_0_.1), channel_id=1, source_target_pairs={{0,2},{1,3},{2,0},{3,1},{4,6},{5,7},{6,4},{7,5},{8,10},{9,11},{10,... | collective-permute-start | bytes 1572872 | tf_op jit(solution)/shard_map/ppermute | solution.py:231
  3.0 1.5 %multiply_reduce_fusion = (f32[128]{0:T(128)S(1)}, f32[128,256]{1,0:T(8,128)S(1)}) fusion(bf16[128,2048]{1,0:T(8,128)(2,1)} %refs_0_.1, bf16[2048,256]{1,0:T(8,128)(2,1)S(1)} %copy-done), kind=kOutput, calls=%fused_computation.2 | convolution fusion | flops 134283136 | bytes 1704448 | tf_op jit(solution)/shard_map/dot_general | solution.py:240
  4.6 0.7 %collective-permute-start.5 = (bf16[128,256]{1,0:T(8,128)(2,1)S(1)}, bf16[128,256]{1,0:T(8,128)(2,1)S(1)}, u32[]{:S(2)}, u32[]{:S(2)}) collective-permute-start(bf16[128,256]{1,0:T(8,128)(2,1)S(1)} %multiply_convert_fusion.own), channel_id=1, source_target_pairs={{0,3},{1,2},{2,1},{3,0},{4,7},{5,6},{6,5},{7,4},{8,11},{9,10},{10,... | collective-permute-start | bytes 196616 | tf_op jit(solution)/shard_map/ppermute | solution.py:231
  5.3 0.6 collective-permute-start.4
  6.6 9.6 %collective-permute-done.1.refs_2_ = bf16[128,2048]{1,0:T(8,128)(2,1)} collective-permute-done((bf16[128,2048]{1,0:T(8,128)(2,1)}, bf16[128,2048]{1,0:T(8,128)(2,1)}, u32[]{:S(2)}, u32[]{:S(2)}) %collective-permute-start.1) | collective-permute-done | bytes 524320 | tf_op jit(solution)/shard_map/ppermute | solution.py:231
  16.2 0.7 %broadcast_in_dim.16 = s32[8,1,128]{2,1,0:T(1,128)} broadcast(s32[8]{0:T(128)S(1)} %select_reduce_fusion), dimensions={0} | broadcast | bytes 4128 | tf_op jit(solution)/shard_map/broadcast_in_dim | solution.py:237
  16.9 6.3 %all-to-all-start = ((s32[8,1,128]{2,1,0:T(1,128)}), s32[8,1,128]{2,1,0:T(1,128)S(1)}, u32[]{:S(2)}, u32[]{:S(2)}) async-start(s32[8,1,128]{2,1,0:T(1,128)} %broadcast_in_dim.16), calls=%async_computation | async-start | bytes 8192 | tf_op jit(solution)/shard_map/all_to_all | solution.py:245
  23.2 6.4 %all-to-all-done.asked = s32[8,1,128]{2,1,0:T(1,128)S(1)} async-done(((s32[8,1,128]{2,1,0:T(1,128)}), s32[8,1,128]{2,1,0:T(1,128)S(1)}, u32[]{:S(2)}, u32[]{:S(2)}) %all-to-all-start) | async-done | bytes 4128 | tf_op jit(solution)/shard_map/all_to_all | solution.py:245
  29.7 1.4 %shard_map.101 = bf16[512,256]{1,0:T(8,128)(2,1)} custom-call(s32[8,1,128]{2,1,0:T(1,128)S(1)} %all-to-all-done.asked, bf16[128,256]{1,0:T(8,128)(2,1)S(1)} %multiply_convert_fusion.own, bf16[128,256]{1,0:T(8,128)(2,1)S(1)} %collective-permute-done.3.core, bf16[128,256]{1,0:T(8,128)(2,1)S(1)} %collective-permute-done.4.far, ...), custom_call_target="tpu_custom_call" | custom-call | bytes 786432 | tf_op jit(solution)/shard_map/pallas_call | solution.py:50
  31.1 4.2 %all-to-all-start.1 = ((bf16[8,64,256]{2,1,0:T(8,128)(2,1)}), bf16[8,64,256]{2,1,0:T(8,128)(2,1)}, u32[]{:S(2)}, u32[]{:S(2)}) async-start(bf16[8,64,256]{2,1,0:T(8,128)(2,1)} %bitcast), calls=%async_computation.1 | async-start | bytes 524288 | tf_op jit(solution)/shard_map/all_to_all | solution.py:266
  35.4 1.6 %collective-permute-start.8 = (bf16[64,2048]{1,0:T(8,128)(2,1)S(1)}, bf16[64,2048]{1,0:T(8,128)(2,1)S(1)}, u32[]{:S(2)}, u32[]{:S(2)}) collective-permute-start(bf16[64,2048]{1,0:T(8,128)(2,1)S(1)} %get-tuple-element.5), channel_id=1, source_target_pairs={{0,2},{1,3},{2,0},{3,1},{4,6},{5,7},{6,4},{7,5},{8,10},{9,11},{10,... | collective-permute-start | bytes 786440 | tf_op jit(solution)/shard_map/ppermute | solution.py:231
  37.5 7.2 %collective-permute-done.8.second = bf16[64,2048]{1,0:T(8,128)(2,1)S(1)} collective-permute-done((bf16[64,2048]{1,0:T(8,128)(2,1)S(1)}, bf16[64,2048]{1,0:T(8,128)(2,1)S(1)}, u32[]{:S(2)}, u32[]{:S(2)}) %collective-permute-start.8) | collective-permute-done | bytes 262176 | tf_op jit(solution)/shard_map/ppermute | solution.py:231
  44.6 1.9 %collective-permute-start.10 = (bf16[64,2048]{1,0:T(8,128)(2,1)S(1)}, bf16[64,2048]{1,0:T(8,128)(2,1)S(1)}, u32[]{:S(2)}, u32[]{:S(2)}) collective-permute-start(bf16[64,2048]{1,0:T(8,128)(2,1)S(1)} %collective-permute-done.8.second), channel_id=1, source_target_pairs={{0,8},{4,12},{8,0},{12,4},{16,24},{20,28},{24,16},{28,20},{1,9},{5... | collective-permute-start | bytes 786440 | tf_op jit(solution)/shard_map/ppermute | solution.py:255
  46.5 1.8 %collective-permute-done.7.first = bf16[64,2048]{1,0:T(8,128)(2,1)S(1)} collective-permute-done((bf16[64,2048]{1,0:T(8,128)(2,1)S(1)}, bf16[64,2048]{1,0:T(8,128)(2,1)S(1)}, u32[]{:S(2)}, u32[]{:S(2)}) %collective-permute-start.7) | collective-permute-done | bytes 262176 | tf_op jit(solution)/shard_map/ppermute | solution.py:231
  48.3 1.6 %collective-permute-start.9 = (bf16[64,2048]{1,0:T(8,128)(2,1)S(1)}, bf16[64,2048]{1,0:T(8,128)(2,1)}, u32[]{:S(2)}, u32[]{:S(2)}) collective-permute-start(bf16[64,2048]{1,0:T(8,128)(2,1)S(1)} %collective-permute-done.7.first), channel_id=1, source_target_pairs={{0,4},{4,0},{8,12},{12,8},{16,20},{20,16},{24,28},{28,24},{1,5},{5... | collective-permute-start | bytes 786440 | tf_op jit(solution)/shard_map/ppermute | solution.py:255
  50.0 2.4 %shard_map.100.absorbed = bf16[4,2,128,256]{3,2,1,0:T(8,128)(2,1)S(1)} custom-call(bf16[128,2048]{1,0:T(8,128)(2,1)S(1)} %copy-done.2, bf16[128,2048]{1,0:T(8,128)(2,1)} %collective-permute-done.refs_1_, bf16[128,2048]{1,0:T(8,128)(2,1)} %collective-permute-done.1.refs_2_, bf16[128,2048]{1,0:T(8,128)(2,1)} %collective-permute-done.2.refs_3_, ...), custom_call_target="tpu_custom_call" | custom-call | flops 536870912 | bytes 3801600 | tf_op jit(solution)/shard_map/pallas_call | solution.py:50
  52.4 0.8 %copy-done.3 = bf16[4,2,128,256]{3,2,1,0:T(8,128)(2,1)} copy-done((bf16[4,2,128,256]{3,2,1,0:T(8,128)(2,1)}, bf16[4,2,128,256]{3,2,1,0:T(8,128)(2,1)S(1)}, u32[]{:S(2)}) %copy-start.3) | copy-done | bytes 524312
  53.2 3.6 %shard_map.103 = bf16[256,256]{1,0:T(8,128)(2,1)} custom-call(s32[8,11]{1,0:T(8,128)} %chosen.3, bf16[4,2,128,256]{3,2,1,0:T(8,128)(2,1)} %copy-done.3, bf16[128,256]{1,0:T(8,128)(2,1)} %copy-done.6, bf16[128,256]{1,0:T(8,128)(2,1)} %copy-done.12, bf16[128,256]{1,0:T(8,128)(2,1)} %copy-done.10, bf16[128,256]{1,0:T(8,128)(2,1)} %copy-done.8, ...), custom_call_target="tpu_custom_call" | custom-call | flops 738197504 | bytes 3670528 | tf_op jit(solution)/shard_map/pallas_call | solution.py:50
  56.8 1.5 %collective-permute-start.6 = (bf16[256,256]{1,0:T(8,128)(2,1)}, bf16[256,256]{1,0:T(8,128)(2,1)S(1)}, u32[]{:S(2)}, u32[]{:S(2)}) collective-permute-start(bf16[256,256]{1,0:T(8,128)(2,1)} %shard_map.103), channel_id=1, source_target_pairs={{0,2},{1,3},{2,0},{3,1},{4,6},{5,7},{6,4},{7,5},{8,10},{9,11},{10,... | collective-permute-start | bytes 393224 | tf_op jit(solution)/shard_map/ppermute | solution.py:231
  58.4 2.9 %shard_map.102.near = bf16[256,2048]{1,0:T(8,128)(2,1)S(1)} custom-call(s32[8,11]{1,0:T(8,128)S(1)} %copy-done.17, bf16[4,2,128,256]{3,2,1,0:T(8,128)(2,1)S(1)} %copy-done.4, bf16[128,256]{1,0:T(8,128)(2,1)S(1)} %copy-done.7, bf16[128,256]{1,0:T(8,128)(2,1)S(1)} %copy-done.13, bf16[128,256]{1,0:T(8,128)(2,1)S(1)} %copy-done.11, ...), custom_call_target="tpu_custom_call" | custom-call | flops 738197504 | bytes 5636608 | tf_op jit(solution)/shard_map/pallas_call | solution.py:50
  61.4 0.6 collective-permute-done.6.far
  62.0 1.4 %shard_map.105 = bf16[128,2048]{1,0:T(8,128)(2,1)S(1)} custom-call(bf16[256,2048]{1,0:T(8,128)(2,1)S(1)} %shard_map.102.near, bf16[256,256]{1,0:T(8,128)(2,1)S(1)} %collective-permute-done.6.far, bf16[64,2048]{1,0:T(8,128)(2,1)S(1)} %collective-permute-done.7.first, bf16[64,2048]{1,0:T(8,128)(2,1)S(1)} %collective-permute-done.8.second, ...), custom_call_target="tpu_custom_call" | custom-call | flops 134217728 | bytes 2752512 | tf_op jit(solution)/shard_map/pallas_call | solution.py:50
  63.4 1.4 %shard_map.104 = f32[128,2048]{1,0:T(8,128)S(1)} custom-call(bf16[256,2048]{1,0:T(8,128)(2,1)S(1)} %shard_map.102.near, bf16[256,256]{1,0:T(8,128)(2,1)S(1)} %collective-permute-done.6.far, bf16[64,2048]{1,0:T(8,128)(2,1)S(1)} %collective-permute-done.7.first, bf16[64,2048]{1,0:T(8,128)(2,1)S(1)} %collective-permute-done.8.second, ...), custom_call_target="tpu_custom_call" | custom-call | flops 134217728 | bytes 2752512 | tf_op jit(solution)/shard_map/pallas_call | solution.py:50
  65.3 0.9 %add_convert_fusion = bf16[128,2048]{1,0:T(8,128)(2,1)} fusion(f32[128,2048]{1,0:T(8,128)S(1)} %shard_map.104, bf16[128,2048]{1,0:T(8,128)(2,1)S(1)} %collective-permute-done.11), kind=kLoop, calls=%fused_computation | loop fusion | flops 786432 | bytes 2097152 | tf_op jit(solution)/shard_map/convert_element_type | solution.py:314
  (61 shorter events, 2.1 us)
Async XLA Ops:
  0.0 6.5 %copy-start.2 = (bf16[128,2048]{1,0:T(8,128)(2,1)S(1)}, bf16[128,2048]{1,0:T(8,128)(2,1)}, u32[]{:S(2)}) copy-start(bf16[128,2048]{1,0:T(8,128)(2,1)} %refs_0_.1) | copy-start | bytes 1572868
  0.0 16.1 %collective-permute-start.1 = (bf16[128,2048]{1,0:T(8,128)(2,1)}, bf16[128,2048]{1,0:T(8,128)(2,1)}, u32[]{:S(2)}, u32[]{:S(2)}) collective-permute-start(bf16[128,2048]{1,0:T(8,128)(2,1)} %refs_0_.1), channel_id=1, source_target_pairs={{0,2},{1,3},{2,0},{3,1},{4,6},{5,7},{6,4},{7,5},{8,10},{9,11},{10,... | collective-permute-start | bytes 1572872 | tf_op jit(solution)/shard_map/ppermute | solution.py:231
  4.5 30.8 %copy-start.1 = (bf16[256,2048]{1,0:T(8,128)(2,1)S(1)}, bf16[256,2048]{1,0:T(8,128)(2,1)}, u32[]{:S(2)}) copy-start(bf16[256,2048]{1,0:T(8,128)(2,1)} %rest_0_.1) | copy-start | bytes 3145732
  4.6 26.4 %copy-start.6 = (bf16[128,256]{1,0:T(8,128)(2,1)}, bf16[128,256]{1,0:T(8,128)(2,1)S(1)}, u32[]{:S(2)}) copy-start(bf16[128,256]{1,0:T(8,128)(2,1)S(1)} %multiply_convert_fusion.own) | copy-start | bytes 196612
  4.6 25.0 %collective-permute-start.5 = (bf16[128,256]{1,0:T(8,128)(2,1)S(1)}, bf16[128,256]{1,0:T(8,128)(2,1)S(1)}, u32[]{:S(2)}, u32[]{:S(2)}) collective-permute-start(bf16[128,256]{1,0:T(8,128)(2,1)S(1)} %multiply_convert_fusion.own), channel_id=1, source_target_pairs={{0,3},{1,2},{2,1},{3,0},{4,7},{5,6},{6,5},{7,4},{8,11},{9,10},{10,... | collective-permute-start | bytes 196616 | tf_op jit(solution)/shard_map/ppermute | solution.py:231
  5.3 24.3 %collective-permute-start.4 = (bf16[128,256]{1,0:T(8,128)(2,1)S(1)}, bf16[128,256]{1,0:T(8,128)(2,1)S(1)}, u32[]{:S(2)}, u32[]{:S(2)}) collective-permute-start(bf16[128,256]{1,0:T(8,128)(2,1)S(1)} %multiply_convert_fusion.own), channel_id=1, source_target_pairs={{0,2},{1,3},{2,0},{3,1},{4,6},{5,7},{6,4},{7,5},{8,10},{9,11},{10,... | collective-permute-start | bytes 196616 | tf_op jit(solution)/shard_map/ppermute | solution.py:231
  6.0 23.7 %collective-permute-start.3 = (bf16[128,256]{1,0:T(8,128)(2,1)S(1)}, bf16[128,256]{1,0:T(8,128)(2,1)S(1)}, u32[]{:S(2)}, u32[]{:S(2)}) collective-permute-start(bf16[128,256]{1,0:T(8,128)(2,1)S(1)} %multiply_convert_fusion.own), channel_id=1, source_target_pairs={{0,1},{1,0},{2,3},{3,2},{4,5},{5,4},{6,7},{7,6},{8,9},{9,8},{10,11... | collective-permute-start | bytes 196616 | tf_op jit(solution)/shard_map/ppermute | solution.py:231
  6.5 43.4 %collective-permute-start = (bf16[128,2048]{1,0:T(8,128)(2,1)S(1)}, bf16[128,2048]{1,0:T(8,128)(2,1)}, u32[]{:S(2)}, u32[]{:S(2)}) collective-permute-start(bf16[128,2048]{1,0:T(8,128)(2,1)S(1)} %copy-done.2), channel_id=1, source_target_pairs={{0,1},{1,0},{2,3},{3,2},{4,5},{5,4},{6,7},{7,6},{8,9},{9,8},{10,11... | collective-permute-start | bytes 1572872 | tf_op jit(solution)/shard_map/ppermute | solution.py:231
  16.1 33.8 %collective-permute-start.2 = (bf16[128,2048]{1,0:T(8,128)(2,1)}, bf16[128,2048]{1,0:T(8,128)(2,1)}, u32[]{:S(2)}, u32[]{:S(2)}) collective-permute-start(bf16[128,2048]{1,0:T(8,128)(2,1)} %collective-permute-done.1.refs_2_), channel_id=1, source_target_pairs={{0,1},{1,0},{2,3},{3,2},{4,5},{5,4},{6,7},{7,6},{8,9},{9,8},{10,11... | collective-permute-start | bytes 1572872 | tf_op jit(solution)/shard_map/ppermute | solution.py:231
  16.9 12.7 %all-to-all-start = ((s32[8,1,128]{2,1,0:T(1,128)}), s32[8,1,128]{2,1,0:T(1,128)S(1)}, u32[]{:S(2)}, u32[]{:S(2)}) async-start(s32[8,1,128]{2,1,0:T(1,128)} %broadcast_in_dim.16), calls=%async_computation | async-start | bytes 8192 | tf_op jit(solution)/shard_map/all_to_all | solution.py:245
  31.1 18.9 %copy-start.14 = (bf16[2,128,256]{2,1,0:T(8,128)(2,1)S(1)}, bf16[2,128,256]{2,1,0:T(8,128)(2,1)}, u32[]{:S(2)}) copy-start(bf16[2,128,256]{2,1,0:T(8,128)(2,1)} %refs_5_.1) | copy-start | bytes 393220
  31.1 22.1 %all-to-all-start.1 = ((bf16[8,64,256]{2,1,0:T(8,128)(2,1)}), bf16[8,64,256]{2,1,0:T(8,128)(2,1)}, u32[]{:S(2)}, u32[]{:S(2)}) async-start(bf16[8,64,256]{2,1,0:T(8,128)(2,1)} %bitcast), calls=%async_computation.1 | async-start | bytes 524288 | tf_op jit(solution)/shard_map/all_to_all | solution.py:266
  35.3 14.7 %copy-start.5 = (bf16[2048,256]{1,0:T(8,128)(2,1)S(1)}, bf16[2048,256]{1,0:T(8,128)(2,1)}, u32[]{:S(2)}) copy-start(bf16[2048,256]{1,0:T(8,128)(2,1)} %refs_4_.1) | copy-start | bytes 3145732
  35.4 14.6 %copy-start.18 = (bf16[256]{0:T(256)(128)(2,1)S(1)}, bf16[256]{0:T(256)(128)(2,1)}, u32[]{:S(2)}) copy-start(bf16[256]{0:T(256)(128)(2,1)} %refs_6_.1) | copy-start | bytes 1540
  35.4 9.2 %collective-permute-start.8 = (bf16[64,2048]{1,0:T(8,128)(2,1)S(1)}, bf16[64,2048]{1,0:T(8,128)(2,1)S(1)}, u32[]{:S(2)}, u32[]{:S(2)}) collective-permute-start(bf16[64,2048]{1,0:T(8,128)(2,1)S(1)} %get-tuple-element.5), channel_id=1, source_target_pairs={{0,2},{1,3},{2,0},{3,1},{4,6},{5,7},{6,4},{7,5},{8,10},{9,11},{10,... | collective-permute-start | bytes 786440 | tf_op jit(solution)/shard_map/ppermute | solution.py:231
  37.0 11.4 %collective-permute-start.7 = (bf16[64,2048]{1,0:T(8,128)(2,1)S(1)}, bf16[64,2048]{1,0:T(8,128)(2,1)S(1)}, u32[]{:S(2)}, u32[]{:S(2)}) collective-permute-start(bf16[64,2048]{1,0:T(8,128)(2,1)S(1)} %get-tuple-element.6), channel_id=1, source_target_pairs={{0,2},{1,3},{2,0},{3,1},{4,6},{5,7},{6,4},{7,5},{8,10},{9,11},{10,... | collective-permute-start | bytes 786440 | tf_op jit(solution)/shard_map/ppermute | solution.py:231
  44.6 16.7 %collective-permute-start.10 = (bf16[64,2048]{1,0:T(8,128)(2,1)S(1)}, bf16[64,2048]{1,0:T(8,128)(2,1)S(1)}, u32[]{:S(2)}, u32[]{:S(2)}) collective-permute-start(bf16[64,2048]{1,0:T(8,128)(2,1)S(1)} %collective-permute-done.8.second), channel_id=1, source_target_pairs={{0,8},{4,12},{8,0},{12,4},{16,24},{20,28},{24,16},{28,20},{1,9},{5... | collective-permute-start | bytes 786440 | tf_op jit(solution)/shard_map/ppermute | solution.py:255
  48.3 13.0 %collective-permute-start.9 = (bf16[64,2048]{1,0:T(8,128)(2,1)S(1)}, bf16[64,2048]{1,0:T(8,128)(2,1)}, u32[]{:S(2)}, u32[]{:S(2)}) collective-permute-start(bf16[64,2048]{1,0:T(8,128)(2,1)S(1)} %collective-permute-done.7.first), channel_id=1, source_target_pairs={{0,4},{4,0},{8,12},{12,8},{16,20},{20,16},{24,28},{28,24},{1,5},{5... | collective-permute-start | bytes 786440 | tf_op jit(solution)/shard_map/ppermute | solution.py:255
  53.1 5.2 %copy-start.4 = (bf16[4,2,128,256]{3,2,1,0:T(8,128)(2,1)S(1)}, bf16[4,2,128,256]{3,2,1,0:T(8,128)(2,1)}, u32[]{:S(2)}) copy-start(bf16[4,2,128,256]{3,2,1,0:T(8,128)(2,1)} %copy-done.3) | copy-start | bytes 1572868
  53.2 5.2 %copy-start.7 = (bf16[128,256]{1,0:T(8,128)(2,1)S(1)}, bf16[128,256]{1,0:T(8,128)(2,1)}, u32[]{:S(2)}) copy-start(bf16[128,256]{1,0:T(8,128)(2,1)} %copy-done.6) | copy-start | bytes 196612
  53.2 5.2 %copy-start.9 = (bf16[128,256]{1,0:T(8,128)(2,1)S(1)}, bf16[128,256]{1,0:T(8,128)(2,1)}, u32[]{:S(2)}) copy-start(bf16[128,256]{1,0:T(8,128)(2,1)} %copy-done.8) | copy-start | bytes 196612
  53.2 5.2 %copy-start.11 = (bf16[128,256]{1,0:T(8,128)(2,1)S(1)}, bf16[128,256]{1,0:T(8,128)(2,1)}, u32[]{:S(2)}) copy-start(bf16[128,256]{1,0:T(8,128)(2,1)} %copy-done.10) | copy-start | bytes 196612
  56.8 5.2 %collective-permute-start.6 = (bf16[256,256]{1,0:T(8,128)(2,1)}, bf16[256,256]{1,0:T(8,128)(2,1)S(1)}, u32[]{:S(2)}, u32[]{:S(2)}) collective-permute-start(bf16[256,256]{1,0:T(8,128)(2,1)} %shard_map.103), channel_id=1, source_target_pairs={{0,2},{1,3},{2,0},{3,1},{4,6},{5,7},{6,4},{7,5},{8,10},{9,11},{10,... | collective-permute-start | bytes 393224 | tf_op jit(solution)/shard_map/ppermute | solution.py:231
  63.4 2.0 %collective-permute-start.11 = (bf16[128,2048]{1,0:T(8,128)(2,1)S(1)}, bf16[128,2048]{1,0:T(8,128)(2,1)S(1)}, u32[]{:S(2)}, u32[]{:S(2)}) collective-permute-start(bf16[128,2048]{1,0:T(8,128)(2,1)S(1)} %shard_map.105), channel_id=1, source_target_pairs={{0,1},{1,0},{2,3},{3,2},{4,5},{5,4},{6,7},{7,6},{8,9},{9,8},{10,11... | collective-permute-start | bytes 1572872 | tf_op jit(solution)/shard_map/ppermute | solution.py:231
  (11 other events, 33.8 us)

commit v3 on v2

--- a/solution.py
+++ b/solution.py
@@ -15,9 +15,9 @@
 VMEM = pl.BlockSpec(memory_space=pltpu.VMEM)
 SLACK = 2
 LANES = 128
-ABSORB = 8 << 20
-FAR = 54 << 20
-NEAR = 46 << 20
+ABSORB = 60 << 20
+FAR = 53 << 20
+NEAR = 8 << 20
 HBM = pl.BlockSpec(memory_space=pl.ANY)
 SMEM = pl.BlockSpec(memory_space=pltpu.SMEM)
 
@@ -46,18 +46,30 @@
         held = [array for array, spec in zip(arrays, in_specs) if spec is VMEM]
         held += list(out_shape) if many else [out_shape]
         held += [array for array in scratch if hasattr(array, "shape")]
-        size = sum(math.prod(array.shape) * 2 for array in held)
+        size = sum(math.prod(array.shape) * array.dtype.itemsize for array in held)
         return pl.pallas_call(
             kernel,
             out_shape=out_shape,
             in_specs=in_specs,
             out_specs=[VMEM] * len(out_shape) if many else VMEM,
             scratch_shapes=list(scratch),
-            compiler_params=pltpu.CompilerParams(vmem_limit_bytes=grant or size + (SLACK << 20)),
+            compiler_params=pltpu.CompilerParams(vmem_limit_bytes=max(grant or 0, size + (SLACK << 20))),
             cost_estimate=pl.CostEstimate(flops=flops, bytes_accessed=size, transcendentals=0),
         )(*arrays)
 
     return run
+
+
+def wanted_kernel(block_count, chosen, wanted):
+    owner, within = split(chosen[...], block_count)
+    within = within.astype(f32)
+
+    def one(index, carry):
+        found = jnp.max(jnp.where(owner == index, within, 0.0))
+        wanted[index] = jnp.full((1, LANES), found, f32).astype(jnp.int32)
+        return carry
+
+    lax.fori_loop(0, wanted.shape[0], one, 0, unroll=8)
 
 
 def pick_kernel(per_shard, asked, own, core, far, diag, outgoing, table):
@@ -97,7 +109,7 @@
 def attend_kernel(
     groups, chosen, absorbed, own, core, far, diag, arrived, value_absorb, head_gain, *rest
 ):
-    out, store, keys, mixed = rest[-4:]
+    outs, (store, keys, mixed) = rest[:-3], rest[-3:]
     me, span = lax.axis_index("tp"), lax.axis_index("kv")
     block_count, picks = chosen.shape
     _, heads, rows, latent_width = absorbed.shape
@@ -184,9 +196,12 @@
         values = jnp.dot(mixed[head], value_absorb[head], preferred_element_type=f32)
         parts.append(rms(values, head_gain[pl.ds(head, 1)].astype(f32)).astype(bf16))
     head_out = jnp.concatenate(parts, axis=1)
-    for weight in rest[:-4]:
-        head_out = jnp.dot(head_out, weight[...], preferred_element_type=f32).astype(bf16)
-    out[...] = head_out
+    if outs[-1].shape[0] == rows:
+        for slot, out in enumerate(outs):
+            out[...] = head_out[slot * rows : (slot + 1) * rows]
+    else:
+        weight, out = outs
+        out[...] = jnp.dot(head_out, weight[...], preferred_element_type=f32).astype(bf16)
 
 
 def project_kernel(half, near, far, first, second, third, fourth, out):
@@ -199,8 +214,8 @@
     relayed = jnp.concatenate([third[...], fourth[...]], axis=0)
     at = pl.multiple_of(parity * depth, depth)
     other = pl.multiple_of((1 - parity) * depth, depth)
-    partial = jnp.dot(far[here, pl.ds(at, depth)], direct, preferred_element_type=f32)
-    partial += jnp.dot(far[here, pl.ds(other, depth)], relayed, preferred_element_type=f32)
+    partial = jnp.dot(far[:, pl.ds(at, depth)], direct, preferred_element_type=f32)
+    partial += jnp.dot(far[:, pl.ds(other, depth)], relayed, preferred_element_type=f32)
     total = near[here].astype(f32) + partial.astype(bf16).astype(f32)
     out[...] = total.astype(out.dtype)
 
@@ -230,12 +245,9 @@
     def swap(array, step):
         return lax.ppermute(array, "tp", [(i, i ^ step) for i in range(shards)])
 
-    owner_of = chosen // block_count
-    within = chosen % block_count
-    matches = owner_of[:, :, None] == jnp.arange(spans, dtype=jnp.int32)[None, None, :]
-    wanted = jnp.max(jnp.where(matches, within[:, :, None], 0), axis=(0, 1))
-    wanted = jnp.broadcast_to(wanted[:, None, None], (spans, 1, LANES))
-
+    wanted = call(
+        functools.partial(wanted_kernel, block_count), shape((spans, 1, LANES), jnp.int32), [VMEM]
+    )(chosen)
     own = rms(
         jnp.dot(tokens, latent_weight, preferred_element_type=f32), latent_gain.astype(f32)
     ).astype(bf16)
@@ -248,8 +260,9 @@
     tokens_diag = swap(tokens_far, 1)
     parity = jnp.bitwise_and(lax.axis_index("kv") ^ (lax.axis_index("kv") >> 1), 1)
     quarter = out_weight.shape[0] // 4
-    piece_a = lax.dynamic_slice(out_weight, (2 * quarter * parity, 0), (quarter, model))
-    piece_b = lax.dynamic_slice(out_weight, (2 * quarter * parity + quarter, 0), (quarter, model))
+    start = 2 * quarter * parity
+    piece_a = lax.dynamic_slice(out_weight, (start, 0), (quarter, model))
+    piece_b = lax.dynamic_slice(out_weight, (start + quarter, 0), (quarter, model))
 
     def relay(array, step):
         return lax.ppermute(array, "kv", [(i, i ^ step) for i in range(spans)])
@@ -285,7 +298,9 @@
     def attend(groups, grant=None, weight=()):
         return call(
             functools.partial(attend_kernel, groups),
-            shape((len(groups) * rows, model if weight else heads * width), bf16),
+            shape((len(groups) * rows, model), bf16)
+            if weight
+            else [shape((rows, heads * width), bf16)] * len(groups),
             [SMEM] + [VMEM] * (8 + len(weight)),
             scratch=[
                 pltpu.VMEM(((block_count + spans) * block_len, latent_width), bf16),
@@ -296,11 +311,12 @@
             grant=grant,
         )(chosen, queries, own, core, far, diag, arrived, value_absorb, head_gain, *weight)
 
-    far_heads = attend((2, 3), FAR)
-    far_heads = swap(far_heads, 2)
+    far_own, far_core = attend((2, 3), FAR)
+    far_core = swap(far_core, 2)
+    far_own = swap(far_own, 2)
     near_part = attend((0, 1), NEAR, (out_weight,))
 
-    def project(half, dtype):
+    def project(half, far_heads, dtype):
         return call(
             functools.partial(project_kernel, half),
             shape((rows, model), dtype),
@@ -308,9 +324,9 @@
             flops=2 * rows * heads * width * model,
         )(near_part, far_heads, *far_weights)
 
-    core_part = project(1, bf16)
+    core_part = project(1, far_core, bf16)
     core_part = swap(core_part, 1)
-    own_part = project(0, f32)
+    own_part = project(0, far_own, f32)
     return (own_part + core_part.astype(f32)).astype(bf16)
 
 

time: 66.7 us -> 63.5 us (0.952)
  waiting for transfers between devices: 26.1 us -> 19.8 us
  local copies, waits for them, and re-layouts: 1.6 us -> 4.1 us
  starting transfers between devices: 22.5 us -> 24.5 us
  Pallas kernels: 13.1 us -> 12 us
    ppermute x10 -> x11, waiting for transfers between devices: 19.7 us -> 13.4 us  [swap(): return lax.ppermute(array, 'tp', [(i, i ^ step) for i in range(shards)])]
    unnamed x42 -> x24, local copies, waits for them, and re-layouts: 0.88 us -> 4.05 us
    ppermute x10 -> x11, starting transfers between devices: 8.62 us -> 10.3 us  [swap(): return lax.ppermute(array, 'tp', [(i, i ^ step) for i in range(shards)])]
    pallas_call x6 -> x7, Pallas kernels: 13.1 us -> 12 us  [run(): pl.pallas_call(kernel, out_shape=out_shape, in_specs=in_specs, out_specs=...]
    broadcast_in_dim x1 -> x0, local copies, waits for them, and re-layouts: 0.67 us -> none  [body(): wanted = jnp.broadcast_to(wanted[:, None, None], (spans, 1, LANES))]
  transfers between devices with their start and end apart: 14 -> 15, of which waited for: 6 -> 5; matrix products, arithmetic and copies ran while one was open for 4% -> 3% of each run, Pallas kernels for 18% -> 18%
where the time goes in v3:
time: 63.5 us; the launch traced here: 63.1 us
  starting transfers between devices  24.5 us (39%)
  waiting for transfers between devices  19.8 us (31%)
  Pallas kernels  12 us (19%)
  local copies, waits for them, and re-layouts  4.1 us (6%)
  matrix products  1.46 us (2%)
  other arithmetic  1 us (2%)
    ppermute x11, waiting for transfers between devices, swap(): return lax.ppermute(array, 'tp', [(i, i ^ step) for i in range(shards)])  13.4 us
    pallas_call x7, Pallas kernels, run(): pl.pallas_call(kernel, out_shape=out_shape, in_specs=in_specs, out_specs=...  12 us
    ppermute x11, starting transfers between devices, swap(): return lax.ppermute(array, 'tp', [(i, i ^ step) for i in range(shards)])  10.3 us
    all_to_all x1, waiting for transfers between devices, body(): lax.all_to_all(wanted, 'kv', split_axis=0, concat_axis=0, tiled=True)  6.4 us
    all_to_all x1, starting transfers between devices, body(): lax.all_to_all(wanted, 'kv', split_axis=0, concat_axis=0, tiled=True)  5.8 us
    all_to_all x1, starting transfers between devices, body(): lax.all_to_all(outgoing.reshape(spans, block_len, latent_width), 'kv', sp...  4.47 us
    unnamed x24, local copies, waits for them, and re-layouts  4.05 us
    ppermute x2, starting transfers between devices, relay(): return lax.ppermute(array, 'kv', [(i, i ^ step) for i in range(spans)])  3.9 us
  transfers between devices with their start and end apart: 15, of which 5 were waited for; matrix products, arithmetic and copies ran while one was open for 3% of the time, Pallas kernels for 18%

profile of v3, /device:TPU:0, one launch (start us, length us, event | category | flops | bytes accessed | tf_op | source)
XLA Modules:
  0.0 63.1 jit_solution(16908547718994238449)
XLA Ops:
  0.0 3.0 %collective-permute-start.1 = (bf16[128,2048]{1,0:T(8,128)(2,1)}, bf16[128,2048]{1,0:T(8,128)(2,1)}, u32[]{:S(2)}, u32[]{:S(2)}) collective-permute-start(bf16[128,2048]{1,0:T(8,128)(2,1)} %refs_0_.1), channel_id=1, source_target_pairs={{0,2},{1,3},{2,0},{3,1},{4,6},{5,7},{6,4},{7,5},{8,10},{9,11},{10,... | collective-permute-start | bytes 1572872 | tf_op jit(solution)/shard_map/ppermute | solution.py:246
  3.0 1.5 %multiply_reduce_fusion = (f32[128]{0:T(128)S(1)}, f32[128,256]{1,0:T(8,128)S(1)}) fusion(bf16[128,2048]{1,0:T(8,128)(2,1)} %refs_0_.1, bf16[2048,256]{1,0:T(8,128)(2,1)S(1)} %copy-done), kind=kOutput, calls=%fused_computation.2 | convolution fusion | flops 134283136 | bytes 1704448 | tf_op jit(solution)/shard_map/dot_general | solution.py:252
  4.6 0.7 %collective-permute-start.5 = (bf16[128,256]{1,0:T(8,128)(2,1)S(1)}, bf16[128,256]{1,0:T(8,128)(2,1)S(1)}, u32[]{:S(2)}, u32[]{:S(2)}) collective-permute-start(bf16[128,256]{1,0:T(8,128)(2,1)S(1)} %multiply_convert_fusion.own), channel_id=1, source_target_pairs={{0,3},{1,2},{2,1},{3,0},{4,7},{5,6},{6,5},{7,4},{8,11},{9,10},{10,... | collective-permute-start | bytes 196616 | tf_op jit(solution)/shard_map/ppermute | solution.py:246
  6.5 0.7 %shard_map.101 = s32[8,1,128]{2,1,0:T(1,128)} custom-call(s32[8,11]{1,0:T(8,128)S(1)} %copy-done.8), custom_call_target="tpu_custom_call" | custom-call | bytes 4448 | tf_op jit(solution)/shard_map/pallas_call | solution.py:50
  7.3 5.8 %all-to-all-start = ((s32[8,1,128]{2,1,0:T(1,128)}), s32[8,1,128]{2,1,0:T(1,128)S(1)}, u32[]{:S(2)}, u32[]{:S(2)}) async-start(s32[8,1,128]{2,1,0:T(1,128)} %shard_map.101), calls=%async_computation | async-start | bytes 8192 | tf_op jit(solution)/shard_map/all_to_all | solution.py:257
  13.1 6.4 %all-to-all-done.asked = s32[8,1,128]{2,1,0:T(1,128)S(1)} async-done(((s32[8,1,128]{2,1,0:T(1,128)}), s32[8,1,128]{2,1,0:T(1,128)S(1)}, u32[]{:S(2)}, u32[]{:S(2)}) %all-to-all-start) | async-done | bytes 4128 | tf_op jit(solution)/shard_map/all_to_all | solution.py:257
  19.5 1.4 %shard_map.102 = bf16[512,256]{1,0:T(8,128)(2,1)} custom-call(s32[8,1,128]{2,1,0:T(1,128)S(1)} %all-to-all-done.asked, bf16[128,256]{1,0:T(8,128)(2,1)S(1)} %multiply_convert_fusion.own, bf16[128,256]{1,0:T(8,128)(2,1)S(1)} %collective-permute-done.3.core, bf16[128,256]{1,0:T(8,128)(2,1)S(1)} %collective-permute-done.4.far, ...), custom_call_target="tpu_custom_call" | custom-call | bytes 786432 | tf_op jit(solution)/shard_map/pallas_call | solution.py:50
  20.9 4.5 %all-to-all-start.1 = ((bf16[8,64,256]{2,1,0:T(8,128)(2,1)}), bf16[8,64,256]{2,1,0:T(8,128)(2,1)S(1)}, u32[]{:S(2)}, u32[]{:S(2)}) async-start(bf16[8,64,256]{2,1,0:T(8,128)(2,1)} %bitcast), calls=%async_computation.1 | async-start | bytes 524288 | tf_op jit(solution)/shard_map/all_to_all | solution.py:279
  25.5 1.6 %collective-permute-start.8 = (bf16[64,2048]{1,0:T(8,128)(2,1)S(1)}, bf16[64,2048]{1,0:T(8,128)(2,1)S(1)}, u32[]{:S(2)}, u32[]{:S(2)}) collective-permute-start(bf16[64,2048]{1,0:T(8,128)(2,1)S(1)} %get-tuple-element.9), channel_id=1, source_target_pairs={{0,2},{1,3},{2,0},{3,1},{4,6},{5,7},{6,4},{7,5},{8,10},{9,11},{10,... | collective-permute-start | bytes 786440 | tf_op jit(solution)/shard_map/ppermute | solution.py:246
  27.6 7.2 %collective-permute-done.8.second = bf16[64,2048]{1,0:T(8,128)(2,1)S(1)} collective-permute-done((bf16[64,2048]{1,0:T(8,128)(2,1)S(1)}, bf16[64,2048]{1,0:T(8,128)(2,1)S(1)}, u32[]{:S(2)}, u32[]{:S(2)}) %collective-permute-start.8) | collective-permute-done | bytes 262176 | tf_op jit(solution)/shard_map/ppermute | solution.py:246
  34.8 1.9 %collective-permute-start.10 = (bf16[64,2048]{1,0:T(8,128)(2,1)S(1)}, bf16[64,2048]{1,0:T(8,128)(2,1)S(1)}, u32[]{:S(2)}, u32[]{:S(2)}) collective-permute-start(bf16[64,2048]{1,0:T(8,128)(2,1)S(1)} %collective-permute-done.8.second), channel_id=1, source_target_pairs={{0,8},{4,12},{8,0},{12,4},{16,24},{20,28},{24,16},{28,20},{1,9},{5... | collective-permute-start | bytes 786440 | tf_op jit(solution)/shard_map/ppermute | solution.py:268
  36.7 3.2 %collective-permute-done.7.first = bf16[64,2048]{1,0:T(8,128)(2,1)S(1)} collective-permute-done((bf16[64,2048]{1,0:T(8,128)(2,1)S(1)}, bf16[64,2048]{1,0:T(8,128)(2,1)S(1)}, u32[]{:S(2)}, u32[]{:S(2)}) %collective-permute-start.7) | collective-permute-done | bytes 262176 | tf_op jit(solution)/shard_map/ppermute | solution.py:246
  39.9 2.0 %collective-permute-start.9 = (bf16[64,2048]{1,0:T(8,128)(2,1)S(1)}, bf16[64,2048]{1,0:T(8,128)(2,1)S(1)}, u32[]{:S(2)}, u32[]{:S(2)}) collective-permute-start(bf16[64,2048]{1,0:T(8,128)(2,1)S(1)} %collective-permute-done.7.first), channel_id=1, source_target_pairs={{0,4},{4,0},{8,12},{12,8},{16,20},{20,16},{24,28},{28,24},{1,5},{5... | collective-permute-start | bytes 786440 | tf_op jit(solution)/shard_map/ppermute | solution.py:268
  41.9 0.8 %copy-done.10 = bf16[128,2048]{1,0:T(8,128)(2,1)} copy-done((bf16[128,2048]{1,0:T(8,128)(2,1)}, bf16[128,2048]{1,0:T(8,128)(2,1)S(1)}, u32[]{:S(2)}) %copy-start.10) | copy-done | bytes 524312
  42.7 3.7 %shard_map.100.absorbed = bf16[4,2,128,256]{3,2,1,0:T(8,128)(2,1)} custom-call(bf16[128,2048]{1,0:T(8,128)(2,1)} %refs_0_.1, bf16[128,2048]{1,0:T(8,128)(2,1)} %collective-permute-done.refs_1_, bf16[128,2048]{1,0:T(8,128)(2,1)} %collective-permute-done.1.refs_2_, bf16[128,2048]{1,0:T(8,128)(2,1)} %copy-done.10, bf16[2048,256]{1,0:T(8,128)(2,1)} %refs_4_.1, ...), custom_call_target="tpu_custom_call" | custom-call | flops 536870912 | bytes 3801600 | tf_op jit(solution)/shard_map/pallas_call | solution.py:50
  47.0 0.8 %copy-done.4 = bf16[128,256]{1,0:T(8,128)(2,1)S(1)} copy-done((bf16[128,256]{1,0:T(8,128)(2,1)S(1)}, bf16[128,256]{1,0:T(8,128)(2,1)}, u32[]{:S(2)}) %copy-start.4) | copy-done | bytes 65560
  47.9 0.8 %copy-done.6 = bf16[128,256]{1,0:T(8,128)(2,1)S(1)} copy-done((bf16[128,256]{1,0:T(8,128)(2,1)S(1)}, bf16[128,256]{1,0:T(8,128)(2,1)}, u32[]{:S(2)}) %copy-start.6) | copy-done | bytes 65560
  48.7 0.9 %copy-done.7 = bf16[2,256,128]{2,1,0:T(8,128)(2,1)S(1)} copy-done((bf16[2,256,128]{2,1,0:T(8,128)(2,1)S(1)}, bf16[2,256,128]{2,1,0:T(8,128)(2,1)}, u32[]{:S(2)}) %copy-start.7) | copy-done | bytes 131096
  49.6 2.7 %shard_map.104 = (bf16[128,256]{1,0:T(8,128)(2,1)S(1)}, bf16[128,256]{1,0:T(8,128)(2,1)S(1)}) custom-call(s32[8,11]{1,0:T(8,128)S(1)} %copy-done.8, bf16[4,2,128,256]{3,2,1,0:T(8,128)(2,1)} %shard_map.100.absorbed, bf16[128,256]{1,0:T(8,128)(2,1)S(1)} %multiply_convert_fusion.own, bf16[128,256]{1,0:T(8,128)(2,1)S(1)} %copy-done.6, ...), custom_call_target="tpu_custom_call" | custom-call | flops 738197504 | bytes 3670528 | tf_op jit(solution)/shard_map/pallas_call | solution.py:50
  52.4 1.6 %collective-permute-start.11 = (bf16[128,256]{1,0:T(8,128)(2,1)S(1)}, bf16[128,256]{1,0:T(8,128)(2,1)S(1)}, u32[]{:S(2)}, u32[]{:S(2)}) collective-permute-start(bf16[128,256]{1,0:T(8,128)(2,1)S(1)} %get-tuple-element.8), channel_id=1, source_target_pairs={{0,2},{1,3},{2,0},{3,1},{4,6},{5,7},{6,4},{7,5},{8,10},{9,11},{10,... | collective-permute-start | bytes 196616 | tf_op jit(solution)/shard_map/ppermute | solution.py:246
  54.0 2.6 %shard_map.103.near = bf16[256,2048]{1,0:T(8,128)(2,1)S(1)} custom-call(s32[8,11]{1,0:T(8,128)S(1)} %copy-done.8, bf16[4,2,128,256]{3,2,1,0:T(8,128)(2,1)S(1)} %copy-done.2, bf16[128,256]{1,0:T(8,128)(2,1)S(1)} %multiply_convert_fusion.own, bf16[128,256]{1,0:T(8,128)(2,1)S(1)} %copy-done.6, bf16[128,256]{1,0:T(8,128)(2,1)S(1)} %copy-done.4, ...), custom_call_target="tpu_custom_call" | custom-call | flops 738197504 | bytes 5636608 | tf_op jit(solution)/shard_map/pallas_call | solution.py:50
  57.2 1.6 %collective-permute-start.6 = (bf16[128,256]{1,0:T(8,128)(2,1)S(1)}, bf16[128,256]{1,0:T(8,128)(2,1)S(1)}, u32[]{:S(2)}, u32[]{:S(2)}) collective-permute-start(bf16[128,256]{1,0:T(8,128)(2,1)S(1)} %get-tuple-element.7), channel_id=1, source_target_pairs={{0,2},{1,3},{2,0},{3,1},{4,6},{5,7},{6,4},{7,5},{8,10},{9,11},{10,... | collective-permute-start | bytes 196616 | tf_op jit(solution)/shard_map/ppermute | solution.py:246
  58.8 2.9 %collective-permute-done.6.far = bf16[128,256]{1,0:T(8,128)(2,1)S(1)} collective-permute-done((bf16[128,256]{1,0:T(8,128)(2,1)S(1)}, bf16[128,256]{1,0:T(8,128)(2,1)S(1)}, u32[]{:S(2)}, u32[]{:S(2)}) %collective-permute-start.6) | collective-permute-done | bytes 65568 | tf_op jit(solution)/shard_map/ppermute | solution.py:246
  62.2 0.9 %add_convert_fusion = bf16[128,2048]{1,0:T(8,128)(2,1)} fusion(f32[128,2048]{1,0:T(8,128)S(1)} %shard_map.105, bf16[128,2048]{1,0:T(8,128)(2,1)S(1)} %collective-permute-done.12), kind=kLoop, calls=%fused_computation | loop fusion | flops 786432 | bytes 2097152 | tf_op jit(solution)/shard_map/convert_element_type | solution.py:330
  (43 shorter events, 3.7 us)
Async XLA Ops:
  0.0 3.0 %copy-start = (bf16[2048,256]{1,0:T(8,128)(2,1)S(1)}, bf16[2048,256]{1,0:T(8,128)(2,1)}, u32[]{:S(2)}) copy-start(bf16[2048,256]{1,0:T(8,128)(2,1)} %param.12) | copy-start | bytes 3145732
  0.0 4.5 %copy-start.11 = (bf16[256]{0:T(256)(128)(2,1)S(1)}, bf16[256]{0:T(256)(128)(2,1)}, u32[]{:S(2)}) copy-start(bf16[256]{0:T(256)(128)(2,1)} %param.15) | copy-start | bytes 1540
  0.0 25.4 %collective-permute-start.1 = (bf16[128,2048]{1,0:T(8,128)(2,1)}, bf16[128,2048]{1,0:T(8,128)(2,1)}, u32[]{:S(2)}, u32[]{:S(2)}) collective-permute-start(bf16[128,2048]{1,0:T(8,128)(2,1)} %refs_0_.1), channel_id=1, source_target_pairs={{0,2},{1,3},{2,0},{3,1},{4,6},{5,7},{6,4},{7,5},{8,10},{9,11},{10,... | collective-permute-start | bytes 1572872 | tf_op jit(solution)/shard_map/ppermute | solution.py:246
  3.0 3.5 %copy-start.8 = (s32[8,11]{1,0:T(8,128)S(1)}, s32[8,11]{1,0:T(8,128)}, u32[]{:S(2)}) copy-start(s32[8,11]{1,0:T(8,128)} %chosen.5) | copy-start | bytes 1060
  4.5 21.0 %copy-start.1 = (bf16[256,2048]{1,0:T(8,128)(2,1)S(1)}, bf16[256,2048]{1,0:T(8,128)(2,1)}, u32[]{:S(2)}) copy-start(bf16[256,2048]{1,0:T(8,128)(2,1)} %rest_0_.1) | copy-start | bytes 3145732
  4.6 14.9 %collective-permute-start.5 = (bf16[128,256]{1,0:T(8,128)(2,1)S(1)}, bf16[128,256]{1,0:T(8,128)(2,1)S(1)}, u32[]{:S(2)}, u32[]{:S(2)}) collective-permute-start(bf16[128,256]{1,0:T(8,128)(2,1)S(1)} %multiply_convert_fusion.own), channel_id=1, source_target_pairs={{0,3},{1,2},{2,1},{3,0},{4,7},{5,6},{6,5},{7,4},{8,11},{9,10},{10,... | collective-permute-start | bytes 196616 | tf_op jit(solution)/shard_map/ppermute | solution.py:246
  5.3 14.2 %collective-permute-start.4 = (bf16[128,256]{1,0:T(8,128)(2,1)S(1)}, bf16[128,256]{1,0:T(8,128)(2,1)S(1)}, u32[]{:S(2)}, u32[]{:S(2)}) collective-permute-start(bf16[128,256]{1,0:T(8,128)(2,1)S(1)} %multiply_convert_fusion.own), channel_id=1, source_target_pairs={{0,2},{1,3},{2,0},{3,1},{4,6},{5,7},{6,4},{7,5},{8,10},{9,11},{10,... | collective-permute-start | bytes 196616 | tf_op jit(solution)/shard_map/ppermute | solution.py:246
  5.9 13.5 %collective-permute-start.3 = (bf16[128,256]{1,0:T(8,128)(2,1)S(1)}, bf16[128,256]{1,0:T(8,128)(2,1)S(1)}, u32[]{:S(2)}, u32[]{:S(2)}) collective-permute-start(bf16[128,256]{1,0:T(8,128)(2,1)S(1)} %multiply_convert_fusion.own), channel_id=1, source_target_pairs={{0,1},{1,0},{2,3},{3,2},{4,5},{5,4},{6,7},{7,6},{8,9},{9,8},{10,11... | collective-permute-start | bytes 196616 | tf_op jit(solution)/shard_map/ppermute | solution.py:246
  7.3 12.2 %all-to-all-start = ((s32[8,1,128]{2,1,0:T(1,128)}), s32[8,1,128]{2,1,0:T(1,128)S(1)}, u32[]{:S(2)}, u32[]{:S(2)}) async-start(s32[8,1,128]{2,1,0:T(1,128)} %shard_map.101), calls=%async_computation | async-start | bytes 8192 | tf_op jit(solution)/shard_map/all_to_all | solution.py:257
  13.1 28.8 %collective-permute-start = (bf16[128,2048]{1,0:T(8,128)(2,1)}, bf16[128,2048]{1,0:T(8,128)(2,1)}, u32[]{:S(2)}, u32[]{:S(2)}) collective-permute-start(bf16[128,2048]{1,0:T(8,128)(2,1)} %refs_0_.1), channel_id=1, source_target_pairs={{0,1},{1,0},{2,3},{3,2},{4,5},{5,4},{6,7},{7,6},{8,9},{9,8},{10,11... | collective-permute-start | bytes 1572872 | tf_op jit(solution)/shard_map/ppermute | solution.py:246
  19.5 1.4 %copy-start.3 = (bf16[128,256]{1,0:T(8,128)(2,1)}, bf16[128,256]{1,0:T(8,128)(2,1)S(1)}, u32[]{:S(2)}) copy-start(bf16[128,256]{1,0:T(8,128)(2,1)S(1)} %collective-permute-done.4.far) | copy-start | bytes 196612
  19.5 1.4 %copy-start.5 = (bf16[128,256]{1,0:T(8,128)(2,1)}, bf16[128,256]{1,0:T(8,128)(2,1)S(1)}, u32[]{:S(2)}) copy-start(bf16[128,256]{1,0:T(8,128)(2,1)S(1)} %collective-permute-done.3.core) | copy-start | bytes 196612
  20.9 25.5 %all-to-all-start.1 = ((bf16[8,64,256]{2,1,0:T(8,128)(2,1)}), bf16[8,64,256]{2,1,0:T(8,128)(2,1)S(1)}, u32[]{:S(2)}, u32[]{:S(2)}) async-start(bf16[8,64,256]{2,1,0:T(8,128)(2,1)} %bitcast), calls=%async_computation.1 | async-start | bytes 524288 | tf_op jit(solution)/shard_map/all_to_all | solution.py:279
  25.4 16.5 %collective-permute-start.2 = (bf16[128,2048]{1,0:T(8,128)(2,1)}, bf16[128,2048]{1,0:T(8,128)(2,1)S(1)}, u32[]{:S(2)}, u32[]{:S(2)}) collective-permute-start(bf16[128,2048]{1,0:T(8,128)(2,1)} %collective-permute-done.1.refs_2_), channel_id=1, source_target_pairs={{0,1},{1,0},{2,3},{3,2},{4,5},{5,4},{6,7},{7,6},{8,9},{9,8},{10,11... | collective-permute-start | bytes 1572872 | tf_op jit(solution)/shard_map/ppermute | solution.py:246
  25.5 9.2 %collective-permute-start.8 = (bf16[64,2048]{1,0:T(8,128)(2,1)S(1)}, bf16[64,2048]{1,0:T(8,128)(2,1)S(1)}, u32[]{:S(2)}, u32[]{:S(2)}) collective-permute-start(bf16[64,2048]{1,0:T(8,128)(2,1)S(1)} %get-tuple-element.9), channel_id=1, source_target_pairs={{0,2},{1,3},{2,0},{3,1},{4,6},{5,7},{6,4},{7,5},{8,10},{9,11},{10,... | collective-permute-start | bytes 786440 | tf_op jit(solution)/shard_map/ppermute | solution.py:246
  27.1 12.8 %collective-permute-start.7 = (bf16[64,2048]{1,0:T(8,128)(2,1)S(1)}, bf16[64,2048]{1,0:T(8,128)(2,1)S(1)}, u32[]{:S(2)}, u32[]{:S(2)}) collective-permute-start(bf16[64,2048]{1,0:T(8,128)(2,1)S(1)} %get-tuple-element.10), channel_id=1, source_target_pairs={{0,2},{1,3},{2,0},{3,1},{4,6},{5,7},{6,4},{7,5},{8,10},{9,11},{10,... | collective-permute-start | bytes 786440 | tf_op jit(solution)/shard_map/ppermute | solution.py:246
  34.8 21.8 %collective-permute-start.10 = (bf16[64,2048]{1,0:T(8,128)(2,1)S(1)}, bf16[64,2048]{1,0:T(8,128)(2,1)S(1)}, u32[]{:S(2)}, u32[]{:S(2)}) collective-permute-start(bf16[64,2048]{1,0:T(8,128)(2,1)S(1)} %collective-permute-done.8.second), channel_id=1, source_target_pairs={{0,8},{4,12},{8,0},{12,4},{16,24},{20,28},{24,16},{28,20},{1,9},{5... | collective-permute-start | bytes 786440 | tf_op jit(solution)/shard_map/ppermute | solution.py:268
  39.9 16.7 %collective-permute-start.9 = (bf16[64,2048]{1,0:T(8,128)(2,1)S(1)}, bf16[64,2048]{1,0:T(8,128)(2,1)S(1)}, u32[]{:S(2)}, u32[]{:S(2)}) collective-permute-start(bf16[64,2048]{1,0:T(8,128)(2,1)S(1)} %collective-permute-done.7.first), channel_id=1, source_target_pairs={{0,4},{4,0},{8,12},{12,8},{16,20},{20,16},{24,28},{28,24},{1,5},{5... | collective-permute-start | bytes 786440 | tf_op jit(solution)/shard_map/ppermute | solution.py:268
  47.0 0.8 %copy-start.4 = (bf16[128,256]{1,0:T(8,128)(2,1)S(1)}, bf16[128,256]{1,0:T(8,128)(2,1)}, u32[]{:S(2)}) copy-start(bf16[128,256]{1,0:T(8,128)(2,1)} %copy-done.3) | copy-start | bytes 196612
  48.7 0.9 %copy-start.7 = (bf16[2,256,128]{2,1,0:T(8,128)(2,1)S(1)}, bf16[2,256,128]{2,1,0:T(8,128)(2,1)}, u32[]{:S(2)}) copy-start(bf16[2,256,128]{2,1,0:T(8,128)(2,1)} %value_absorb.3) | copy-start | bytes 393220
  49.6 4.3 %copy-start.2 = (bf16[4,2,128,256]{3,2,1,0:T(8,128)(2,1)S(1)}, bf16[4,2,128,256]{3,2,1,0:T(8,128)(2,1)}, u32[]{:S(2)}) copy-start(bf16[4,2,128,256]{3,2,1,0:T(8,128)(2,1)} %shard_map.100.absorbed) | copy-start | bytes 1572868
  52.4 4.3 %collective-permute-start.11 = (bf16[128,256]{1,0:T(8,128)(2,1)S(1)}, bf16[128,256]{1,0:T(8,128)(2,1)S(1)}, u32[]{:S(2)}, u32[]{:S(2)}) collective-permute-start(bf16[128,256]{1,0:T(8,128)(2,1)S(1)} %get-tuple-element.8), channel_id=1, source_target_pairs={{0,2},{1,3},{2,0},{3,1},{4,6},{5,7},{6,4},{7,5},{8,10},{9,11},{10,... | collective-permute-start | bytes 196616 | tf_op jit(solution)/shard_map/ppermute | solution.py:246
  57.1 5.0 %collective-permute-start.12 = (bf16[128,2048]{1,0:T(8,128)(2,1)S(1)}, bf16[128,2048]{1,0:T(8,128)(2,1)S(1)}, u32[]{:S(2)}, u32[]{:S(2)}) collective-permute-start(bf16[128,2048]{1,0:T(8,128)(2,1)S(1)} %shard_map.106), channel_id=1, source_target_pairs={{0,1},{1,0},{2,3},{3,2},{4,5},{5,4},{6,7},{7,6},{8,9},{9,8},{10,11... | collective-permute-start | bytes 1572872 | tf_op jit(solution)/shard_map/ppermute | solution.py:246
  57.2 4.5 %collective-permute-start.6 = (bf16[128,256]{1,0:T(8,128)(2,1)S(1)}, bf16[128,256]{1,0:T(8,128)(2,1)S(1)}, u32[]{:S(2)}, u32[]{:S(2)}) collective-permute-start(bf16[128,256]{1,0:T(8,128)(2,1)S(1)} %get-tuple-element.7), channel_id=1, source_target_pairs={{0,2},{1,3},{2,0},{3,1},{4,6},{5,7},{6,4},{7,5},{8,10},{9,11},{10,... | collective-permute-start | bytes 196616 | tf_op jit(solution)/shard_map/ppermute | solution.py:246
  (3 other events, 2.3 us)

commit v4 on v3

--- a/solution.py
+++ b/solution.py
@@ -15,8 +15,8 @@
 VMEM = pl.BlockSpec(memory_space=pltpu.VMEM)
 SLACK = 2
 LANES = 128
-ABSORB = 60 << 20
-FAR = 53 << 20
+ABSORB = 53 << 20
+FAR = 8 << 20
 NEAR = 8 << 20
 HBM = pl.BlockSpec(memory_space=pl.ANY)
 SMEM = pl.BlockSpec(memory_space=pltpu.SMEM)
@@ -91,7 +91,10 @@
 
 
 def absorb_kernel(pieces, *refs):
-    tokens, (query_weight, key_absorb, gain, out) = refs[:pieces], refs[pieces:]
+    tokens, rest = refs[:pieces], refs[pieces:]
+    query_weight, key_absorb, gain, chosen, head_gain, near, far, held, held_gain = rest
+    held[...] = chosen[...]
+    held_gain[...] = head_gain[...]
     heads, width, _ = key_absorb.shape
     scale = gain[...].astype(f32)
     products = [
@@ -101,7 +104,8 @@
         queries = products[piece].astype(bf16)
         for head in range(heads):
             part = queries[:, head * width : (head + 1) * width]
-            out[piece, head] = rms(
+            out, slot = (near, piece) if piece < pieces // 2 else (far, piece - pieces // 2)
+            out[slot, head] = rms(
                 jnp.dot(part, key_absorb[head], preferred_element_type=f32), scale
             ).astype(bf16)
 
@@ -145,7 +149,7 @@
                 pl.ds(pl.multiple_of(source, block_len), block_len)
             ]
             biases.append(jnp.where((target < block) | (pick == 0), 0.0, -jnp.inf).astype(f32))
-        query = absorbed[groups[slot], :, pl.ds(inner * block_len, block_len), :].reshape(
+        query = absorbed[slot, :, pl.ds(inner * block_len, block_len), :].reshape(
             lanes, latent_width
         )
         scores = lax.dot_general(
@@ -287,15 +291,16 @@
     def absorb(pieces):
         return call(
             functools.partial(absorb_kernel, len(pieces)),
-            shape((len(pieces), heads, rows, latent_width), bf16),
-            [VMEM] * (len(pieces) + 3),
+            [shape((len(pieces) // 2, heads, rows, latent_width), bf16)] * 2
+            + [shape(chosen.shape, chosen.dtype), shape(head_gain.shape, bf16)],
+            [VMEM] * (len(pieces) + 5),
             flops=2 * len(pieces) * rows * model * heads * width,
             grant=ABSORB,
-        )(*pieces, query_weight, key_absorb, query_gain)
-
-    queries = absorb([tokens, tokens_core, tokens_far, tokens_diag])
-
-    def attend(groups, grant=None, weight=()):
+        )(*pieces, query_weight, key_absorb, query_gain, chosen, head_gain)
+
+    near_queries, far_queries, held, held_gain = absorb([tokens, tokens_core, tokens_far, tokens_diag])
+
+    def attend(groups, queries, grant=None, weight=()):
         return call(
             functools.partial(attend_kernel, groups),
             shape((len(groups) * rows, model), bf16)
@@ -309,12 +314,12 @@
             ],
             flops=8 * len(groups) * per_shard * heads * block_len * picks * block_len * latent_width,
             grant=grant,
-        )(chosen, queries, own, core, far, diag, arrived, value_absorb, head_gain, *weight)
-
-    far_own, far_core = attend((2, 3), FAR)
+        )(held, queries, own, core, far, diag, arrived, value_absorb, held_gain, *weight)
+
+    far_own, far_core = attend((2, 3), far_queries, FAR)
     far_core = swap(far_core, 2)
     far_own = swap(far_own, 2)
-    near_part = attend((0, 1), NEAR, (out_weight,))
+    near_part = attend((0, 1), near_queries, NEAR, (out_weight,))
 
     def project(half, far_heads, dtype):
         return call(

time: 63.5 us -> 63.9 us (level)
  local copies, waits for them, and re-layouts: 4.1 us -> 5.81 us
  Pallas kernels: 12 us -> 10.6 us
    unnamed x24 -> x34, local copies, waits for them, and re-layouts: 4.05 us -> 5.76 us
    pallas_call x7, Pallas kernels: 12 us -> 10.6 us  [run(): pl.pallas_call(kernel, out_shape=out_shape, in_specs=in_specs, out_specs=...]
  transfers between devices with their start and end apart: 15 -> 15, of which waited for: 5 -> 5; matrix products, arithmetic and copies ran while one was open for 3% -> 3% of each run, Pallas kernels for 18% -> 16%
where the time goes in v4:
time: 63.9 us; the launch traced here: 63.5 us
  starting transfers between devices  24.6 us (38%)
  waiting for transfers between devices  19.7 us (31%)
  Pallas kernels  10.6 us (17%)
  local copies, waits for them, and re-layouts  5.81 us (9%)
  matrix products  1.46 us (2%)
  other arithmetic  1 us (2%)
    ppermute x11, waiting for transfers between devices, swap(): return lax.ppermute(array, 'tp', [(i, i ^ step) for i in range(shards)])  13.3 us
    pallas_call x7, Pallas kernels, run(): pl.pallas_call(kernel, out_shape=out_shape, in_specs=in_specs, out_specs=...  10.6 us
    ppermute x11, starting transfers between devices, swap(): return lax.ppermute(array, 'tp', [(i, i ^ step) for i in range(shards)])  10.3 us
    all_to_all x1, waiting for transfers between devices, body(): lax.all_to_all(wanted, 'kv', split_axis=0, concat_axis=0, tiled=True)  6.4 us
    all_to_all x1, starting transfers between devices, body(): lax.all_to_all(wanted, 'kv', split_axis=0, concat_axis=0, tiled=True)  5.8 us
    unnamed x34, local copies, waits for them, and re-layouts  5.76 us
    all_to_all x1, starting transfers between devices, body(): lax.all_to_all(outgoing.reshape(spans, block_len, latent_width), 'kv', sp...  4.47 us
    ppermute x2, starting transfers between devices, relay(): return lax.ppermute(array, 'kv', [(i, i ^ step) for i in range(spans)])  4.03 us
  transfers between devices with their start and end apart: 15, of which 5 were waited for; matrix products, arithmetic and copies ran while one was open for 3% of the time, Pallas kernels for 16%

profile of v4, /device:TPU:0, one launch (start us, length us, event | category | flops | bytes accessed | tf_op | source)
XLA Modules:
  0.0 63.5 jit_solution(15021891973222727343)
XLA Ops:
  0.0 3.0 %collective-permute-start.1 = (bf16[128,2048]{1,0:T(8,128)(2,1)}, bf16[128,2048]{1,0:T(8,128)(2,1)}, u32[]{:S(2)}, u32[]{:S(2)}) collective-permute-start(bf16[128,2048]{1,0:T(8,128)(2,1)} %refs_0_.1), channel_id=1, source_target_pairs={{0,2},{1,3},{2,0},{3,1},{4,6},{5,7},{6,4},{7,5},{8,10},{9,11},{10,... | collective-permute-start | bytes 1572872 | tf_op jit(solution)/shard_map/ppermute | solution.py:250
  3.0 1.5 %multiply_reduce_fusion = (f32[128]{0:T(128)S(1)}, f32[128,256]{1,0:T(8,128)S(1)}) fusion(bf16[128,2048]{1,0:T(8,128)(2,1)} %refs_0_.1, bf16[2048,256]{1,0:T(8,128)(2,1)S(1)} %copy-done), kind=kOutput, calls=%fused_computation.2 | convolution fusion | flops 134283136 | bytes 1704448 | tf_op jit(solution)/shard_map/dot_general | solution.py:256
  6.5 0.7 %shard_map.101 = s32[8,1,128]{2,1,0:T(1,128)} custom-call(s32[8,11]{1,0:T(8,128)S(1)} %copy-done.10), custom_call_target="tpu_custom_call" | custom-call | bytes 4448 | tf_op jit(solution)/shard_map/pallas_call | solution.py:50
  7.3 5.8 %all-to-all-start = ((s32[8,1,128]{2,1,0:T(1,128)}), s32[8,1,128]{2,1,0:T(1,128)S(1)}, u32[]{:S(2)}, u32[]{:S(2)}) async-start(s32[8,1,128]{2,1,0:T(1,128)} %shard_map.101), calls=%async_computation | async-start | bytes 8192 | tf_op jit(solution)/shard_map/all_to_all | solution.py:261
  13.1 6.4 %all-to-all-done.asked = s32[8,1,128]{2,1,0:T(1,128)S(1)} async-done(((s32[8,1,128]{2,1,0:T(1,128)}), s32[8,1,128]{2,1,0:T(1,128)S(1)}, u32[]{:S(2)}, u32[]{:S(2)}) %all-to-all-start) | async-done | bytes 4128 | tf_op jit(solution)/shard_map/all_to_all | solution.py:261
  19.5 1.4 %shard_map.102 = bf16[512,256]{1,0:T(8,128)(2,1)} custom-call(s32[8,1,128]{2,1,0:T(1,128)S(1)} %all-to-all-done.asked, bf16[128,256]{1,0:T(8,128)(2,1)S(1)} %multiply_convert_fusion.own, bf16[128,256]{1,0:T(8,128)(2,1)S(1)} %collective-permute-done.3.core, bf16[128,256]{1,0:T(8,128)(2,1)S(1)} %collective-permute-done.4.far, ...), custom_call_target="tpu_custom_call" | custom-call | bytes 786432 | tf_op jit(solution)/shard_map/pallas_call | solution.py:50
  20.9 4.5 %all-to-all-start.1 = ((bf16[8,64,256]{2,1,0:T(8,128)(2,1)}), bf16[8,64,256]{2,1,0:T(8,128)(2,1)S(1)}, u32[]{:S(2)}, u32[]{:S(2)}) async-start(bf16[8,64,256]{2,1,0:T(8,128)(2,1)} %bitcast), calls=%async_computation.1 | async-start | bytes 524288 | tf_op jit(solution)/shard_map/all_to_all | solution.py:283
  25.6 1.6 %collective-permute-start.8 = (bf16[64,2048]{1,0:T(8,128)(2,1)S(1)}, bf16[64,2048]{1,0:T(8,128)(2,1)S(1)}, u32[]{:S(2)}, u32[]{:S(2)}) collective-permute-start(bf16[64,2048]{1,0:T(8,128)(2,1)S(1)} %get-tuple-element.17), channel_id=1, source_target_pairs={{0,2},{1,3},{2,0},{3,1},{4,6},{5,7},{6,4},{7,5},{8,10},{9,11},{10,... | collective-permute-start | bytes 786440 | tf_op jit(solution)/shard_map/ppermute | solution.py:250
  27.6 7.2 %collective-permute-done.8.second = bf16[64,2048]{1,0:T(8,128)(2,1)S(1)} collective-permute-done((bf16[64,2048]{1,0:T(8,128)(2,1)S(1)}, bf16[64,2048]{1,0:T(8,128)(2,1)S(1)}, u32[]{:S(2)}, u32[]{:S(2)}) %collective-permute-start.8) | collective-permute-done | bytes 262176 | tf_op jit(solution)/shard_map/ppermute | solution.py:250
  34.8 2.0 %collective-permute-start.10 = (bf16[64,2048]{1,0:T(8,128)(2,1)S(1)}, bf16[64,2048]{1,0:T(8,128)(2,1)S(1)}, u32[]{:S(2)}, u32[]{:S(2)}) collective-permute-start(bf16[64,2048]{1,0:T(8,128)(2,1)S(1)} %collective-permute-done.8.second), channel_id=1, source_target_pairs={{0,8},{4,12},{8,0},{12,4},{16,24},{20,28},{24,16},{28,20},{1,9},{5... | collective-permute-start | bytes 786440 | tf_op jit(solution)/shard_map/ppermute | solution.py:272
  36.8 3.1 %collective-permute-done.7.first = bf16[64,2048]{1,0:T(8,128)(2,1)S(1)} collective-permute-done((bf16[64,2048]{1,0:T(8,128)(2,1)S(1)}, bf16[64,2048]{1,0:T(8,128)(2,1)S(1)}, u32[]{:S(2)}, u32[]{:S(2)}) %collective-permute-start.7) | collective-permute-done | bytes 262176 | tf_op jit(solution)/shard_map/ppermute | solution.py:250
  39.9 2.0 %collective-permute-start.9 = (bf16[64,2048]{1,0:T(8,128)(2,1)S(1)}, bf16[64,2048]{1,0:T(8,128)(2,1)S(1)}, u32[]{:S(2)}, u32[]{:S(2)}) collective-permute-start(bf16[64,2048]{1,0:T(8,128)(2,1)S(1)} %collective-permute-done.7.first), channel_id=1, source_target_pairs={{0,4},{4,0},{8,12},{12,8},{16,20},{20,16},{24,28},{28,24},{1,5},{5... | collective-permute-start | bytes 786440 | tf_op jit(solution)/shard_map/ppermute | solution.py:272
  42.0 0.8 %copy-done.15 = bf16[128,2048]{1,0:T(8,128)(2,1)} copy-done((bf16[128,2048]{1,0:T(8,128)(2,1)}, bf16[128,2048]{1,0:T(8,128)(2,1)S(1)}, u32[]{:S(2)}) %copy-start.15) | copy-done | bytes 524312
  42.8 2.9 %shard_map.100 = (bf16[2,2,128,256]{3,2,1,0:T(8,128)(2,1)S(1)}, bf16[2,2,128,256]{3,2,1,0:T(8,128)(2,1)S(1)}, s32[8,11]{1,0:T(8,128)S(1)}, bf16[2,128]{1,0:T(2,128)(2,1)S(1)}) custom-call(bf16[128,2048]{1,0:T(8,128)(2,1)} %refs_0_.1, bf16[128,2048]{1,0:T(8,128)(2,1)} %collective-permute-done.refs_1_, bf16[128,2048]{1,0:T(8,128)(2,1)} %collective-permute-done.1.refs_2_, ...), custom_call_target="tpu_custom_call" | custom-call | flops 536870912 | bytes 3803328 | tf_op jit(solution)/shard_map/pallas_call | solution.py:50
  47.0 0.8 %copy-done.5 = bf16[128,256]{1,0:T(8,128)(2,1)S(1)} copy-done((bf16[128,256]{1,0:T(8,128)(2,1)S(1)}, bf16[128,256]{1,0:T(8,128)(2,1)}, u32[]{:S(2)}) %copy-start.5) | copy-done | bytes 65560
  47.9 0.8 %copy-done.7 = bf16[128,256]{1,0:T(8,128)(2,1)S(1)} copy-done((bf16[128,256]{1,0:T(8,128)(2,1)S(1)}, bf16[128,256]{1,0:T(8,128)(2,1)}, u32[]{:S(2)}) %copy-start.7) | copy-done | bytes 65560
  48.7 0.9 %copy-done.9 = bf16[2,256,128]{2,1,0:T(8,128)(2,1)S(1)} copy-done((bf16[2,256,128]{2,1,0:T(8,128)(2,1)S(1)}, bf16[2,256,128]{2,1,0:T(8,128)(2,1)}, u32[]{:S(2)}) %copy-start.9) | copy-done | bytes 131096
  49.6 0.9 %copy-done.14 = bf16[2,2,128,256]{3,2,1,0:T(8,128)(2,1)S(1)} copy-done((bf16[2,2,128,256]{3,2,1,0:T(8,128)(2,1)S(1)}, bf16[2,2,128,256]{3,2,1,0:T(8,128)(2,1)}, u32[]{:S(2)}) %copy-start.14) | copy-done | bytes 262168
  50.6 2.2 %shard_map.104 = (bf16[128,256]{1,0:T(8,128)(2,1)S(1)}, bf16[128,256]{1,0:T(8,128)(2,1)S(1)}) custom-call(s32[8,11]{1,0:T(8,128)S(1)} %get-tuple-element.11.chosen, bf16[2,2,128,256]{3,2,1,0:T(8,128)(2,1)S(1)} %copy-done.14, bf16[128,256]{1,0:T(8,128)(2,1)S(1)} %multiply_convert_fusion.own, bf16[128,256]{1,0:T(8,128)(2,1)S(1)} %copy-done.7, ...), custom_call_target="tpu_custom_call" | custom-call | flops 738197504 | bytes 3408384 | tf_op jit(solution)/shard_map/pallas_call | solution.py:50
  52.8 1.6 %collective-permute-start.11 = (bf16[128,256]{1,0:T(8,128)(2,1)S(1)}, bf16[128,256]{1,0:T(8,128)(2,1)S(1)}, u32[]{:S(2)}, u32[]{:S(2)}) collective-permute-start(bf16[128,256]{1,0:T(8,128)(2,1)S(1)} %get-tuple-element.16), channel_id=1, source_target_pairs={{0,2},{1,3},{2,0},{3,1},{4,6},{5,7},{6,4},{7,5},{8,10},{9,11},{10,... | collective-permute-start | bytes 196616 | tf_op jit(solution)/shard_map/ppermute | solution.py:250
  54.4 2.6 %shard_map.103.near = bf16[256,2048]{1,0:T(8,128)(2,1)S(1)} custom-call(s32[8,11]{1,0:T(8,128)S(1)} %get-tuple-element.11.chosen, bf16[2,2,128,256]{3,2,1,0:T(8,128)(2,1)S(1)} %copy-done.3, bf16[128,256]{1,0:T(8,128)(2,1)S(1)} %multiply_convert_fusion.own, bf16[128,256]{1,0:T(8,128)(2,1)S(1)} %copy-done.7, bf16[128,256]{1,0:T(8,128)(2,1)S(1)} %copy-done.5, ...), custom_call_target="tpu_custom_call" | custom-call | flops 738197504 | bytes 5374464 | tf_op jit(solution)/shard_map/pallas_call | solution.py:50
  57.6 1.6 %collective-permute-start.6 = (bf16[128,256]{1,0:T(8,128)(2,1)S(1)}, bf16[128,256]{1,0:T(8,128)(2,1)S(1)}, u32[]{:S(2)}, u32[]{:S(2)}) collective-permute-start(bf16[128,256]{1,0:T(8,128)(2,1)S(1)} %get-tuple-element.15), channel_id=1, source_target_pairs={{0,2},{1,3},{2,0},{3,1},{4,6},{5,7},{6,4},{7,5},{8,10},{9,11},{10,... | collective-permute-start | bytes 196616 | tf_op jit(solution)/shard_map/ppermute | solution.py:250
  59.2 2.9 %collective-permute-done.6.far = bf16[128,256]{1,0:T(8,128)(2,1)S(1)} collective-permute-done((bf16[128,256]{1,0:T(8,128)(2,1)S(1)}, bf16[128,256]{1,0:T(8,128)(2,1)S(1)}, u32[]{:S(2)}, u32[]{:S(2)}) %collective-permute-start.6) | collective-permute-done | bytes 65568 | tf_op jit(solution)/shard_map/ppermute | solution.py:250
  62.6 0.9 %add_convert_fusion = bf16[128,2048]{1,0:T(8,128)(2,1)} fusion(f32[128,2048]{1,0:T(8,128)S(1)} %shard_map.105, bf16[128,2048]{1,0:T(8,128)(2,1)S(1)} %collective-permute-done.12), kind=kLoop, calls=%fused_computation | loop fusion | flops 786432 | bytes 2097152 | tf_op jit(solution)/shard_map/convert_element_type | solution.py:335
  (53 shorter events, 5.2 us)
Async XLA Ops:
  0.0 3.0 %copy-start = (bf16[2048,256]{1,0:T(8,128)(2,1)S(1)}, bf16[2048,256]{1,0:T(8,128)(2,1)}, u32[]{:S(2)}) copy-start(bf16[2048,256]{1,0:T(8,128)(2,1)} %param.12) | copy-start | bytes 3145732
  0.0 4.5 %copy-start.16 = (bf16[256]{0:T(256)(128)(2,1)S(1)}, bf16[256]{0:T(256)(128)(2,1)}, u32[]{:S(2)}) copy-start(bf16[256]{0:T(256)(128)(2,1)} %param.15) | copy-start | bytes 1540
  0.0 25.4 %collective-permute-start.1 = (bf16[128,2048]{1,0:T(8,128)(2,1)}, bf16[128,2048]{1,0:T(8,128)(2,1)}, u32[]{:S(2)}, u32[]{:S(2)}) collective-permute-start(bf16[128,2048]{1,0:T(8,128)(2,1)} %refs_0_.1), channel_id=1, source_target_pairs={{0,2},{1,3},{2,0},{3,1},{4,6},{5,7},{6,4},{7,5},{8,10},{9,11},{10,... | collective-permute-start | bytes 1572872 | tf_op jit(solution)/shard_map/ppermute | solution.py:250
  3.0 3.5 %copy-start.10 = (s32[8,11]{1,0:T(8,128)S(1)}, s32[8,11]{1,0:T(8,128)}, u32[]{:S(2)}) copy-start(s32[8,11]{1,0:T(8,128)} %chosen.1) | copy-start | bytes 1060
  4.5 21.0 %copy-start.1 = (bf16[256,2048]{1,0:T(8,128)(2,1)S(1)}, bf16[256,2048]{1,0:T(8,128)(2,1)}, u32[]{:S(2)}) copy-start(bf16[256,2048]{1,0:T(8,128)(2,1)} %rest_0_.1) | copy-start | bytes 3145732
  4.6 14.9 %collective-permute-start.5 = (bf16[128,256]{1,0:T(8,128)(2,1)S(1)}, bf16[128,256]{1,0:T(8,128)(2,1)S(1)}, u32[]{:S(2)}, u32[]{:S(2)}) collective-permute-start(bf16[128,256]{1,0:T(8,128)(2,1)S(1)} %multiply_convert_fusion.own), channel_id=1, source_target_pairs={{0,3},{1,2},{2,1},{3,0},{4,7},{5,6},{6,5},{7,4},{8,11},{9,10},{10,... | collective-permute-start | bytes 196616 | tf_op jit(solution)/shard_map/ppermute | solution.py:250
  5.3 14.2 %collective-permute-start.4 = (bf16[128,256]{1,0:T(8,128)(2,1)S(1)}, bf16[128,256]{1,0:T(8,128)(2,1)S(1)}, u32[]{:S(2)}, u32[]{:S(2)}) collective-permute-start(bf16[128,256]{1,0:T(8,128)(2,1)S(1)} %multiply_convert_fusion.own), channel_id=1, source_target_pairs={{0,2},{1,3},{2,0},{3,1},{4,6},{5,7},{6,4},{7,5},{8,10},{9,11},{10,... | collective-permute-start | bytes 196616 | tf_op jit(solution)/shard_map/ppermute | solution.py:250
  5.9 13.5 %collective-permute-start.3 = (bf16[128,256]{1,0:T(8,128)(2,1)S(1)}, bf16[128,256]{1,0:T(8,128)(2,1)S(1)}, u32[]{:S(2)}, u32[]{:S(2)}) collective-permute-start(bf16[128,256]{1,0:T(8,128)(2,1)S(1)} %multiply_convert_fusion.own), channel_id=1, source_target_pairs={{0,1},{1,0},{2,3},{3,2},{4,5},{5,4},{6,7},{7,6},{8,9},{9,8},{10,11... | collective-permute-start | bytes 196616 | tf_op jit(solution)/shard_map/ppermute | solution.py:250
  7.3 12.2 %all-to-all-start = ((s32[8,1,128]{2,1,0:T(1,128)}), s32[8,1,128]{2,1,0:T(1,128)S(1)}, u32[]{:S(2)}, u32[]{:S(2)}) async-start(s32[8,1,128]{2,1,0:T(1,128)} %shard_map.101), calls=%async_computation | async-start | bytes 8192 | tf_op jit(solution)/shard_map/all_to_all | solution.py:261
  13.1 28.9 %collective-permute-start = (bf16[128,2048]{1,0:T(8,128)(2,1)}, bf16[128,2048]{1,0:T(8,128)(2,1)}, u32[]{:S(2)}, u32[]{:S(2)}) collective-permute-start(bf16[128,2048]{1,0:T(8,128)(2,1)} %refs_0_.1), channel_id=1, source_target_pairs={{0,1},{1,0},{2,3},{3,2},{4,5},{5,4},{6,7},{7,6},{8,9},{9,8},{10,11... | collective-permute-start | bytes 1572872 | tf_op jit(solution)/shard_map/ppermute | solution.py:250
  19.5 1.4 %copy-start.4 = (bf16[128,256]{1,0:T(8,128)(2,1)}, bf16[128,256]{1,0:T(8,128)(2,1)S(1)}, u32[]{:S(2)}) copy-start(bf16[128,256]{1,0:T(8,128)(2,1)S(1)} %collective-permute-done.4.far) | copy-start | bytes 196612
  20.9 26.1 %all-to-all-start.1 = ((bf16[8,64,256]{2,1,0:T(8,128)(2,1)}), bf16[8,64,256]{2,1,0:T(8,128)(2,1)S(1)}, u32[]{:S(2)}, u32[]{:S(2)}) async-start(bf16[8,64,256]{2,1,0:T(8,128)(2,1)} %bitcast), calls=%async_computation.1 | async-start | bytes 524288 | tf_op jit(solution)/shard_map/all_to_all | solution.py:283
  25.4 17.4 %copy-start.8 = (bf16[2,128,256]{2,1,0:T(8,128)(2,1)S(1)}, bf16[2,128,256]{2,1,0:T(8,128)(2,1)}, u32[]{:S(2)}) copy-start(bf16[2,128,256]{2,1,0:T(8,128)(2,1)} %refs_5_.1) | copy-start | bytes 393220
  25.4 16.6 %collective-permute-start.2 = (bf16[128,2048]{1,0:T(8,128)(2,1)}, bf16[128,2048]{1,0:T(8,128)(2,1)S(1)}, u32[]{:S(2)}, u32[]{:S(2)}) collective-permute-start(bf16[128,2048]{1,0:T(8,128)(2,1)} %collective-permute-done.1.refs_2_), channel_id=1, source_target_pairs={{0,1},{1,0},{2,3},{3,2},{4,5},{5,4},{6,7},{7,6},{8,9},{9,8},{10,11... | collective-permute-start | bytes 1572872 | tf_op jit(solution)/shard_map/ppermute | solution.py:250
  25.5 17.2 %copy-start.11 = (bf16[256]{0:T(256)(128)(2,1)S(1)}, bf16[256]{0:T(256)(128)(2,1)}, u32[]{:S(2)}) copy-start(bf16[256]{0:T(256)(128)(2,1)} %refs_6_.1) | copy-start | bytes 1540
  25.5 17.2 %copy-start.12 = (bf16[2,128]{1,0:T(2,128)(2,1)S(1)}, bf16[2,128]{1,0:T(2,128)(2,1)}, u32[]{:S(2)}) copy-start(bf16[2,128]{1,0:T(2,128)(2,1)} %refs_8_.1) | copy-start | bytes 1540
  25.6 9.2 %collective-permute-start.8 = (bf16[64,2048]{1,0:T(8,128)(2,1)S(1)}, bf16[64,2048]{1,0:T(8,128)(2,1)S(1)}, u32[]{:S(2)}, u32[]{:S(2)}) collective-permute-start(bf16[64,2048]{1,0:T(8,128)(2,1)S(1)} %get-tuple-element.17), channel_id=1, source_target_pairs={{0,2},{1,3},{2,0},{3,1},{4,6},{5,7},{6,4},{7,5},{8,10},{9,11},{10,... | collective-permute-start | bytes 786440 | tf_op jit(solution)/shard_map/ppermute | solution.py:250
  27.1 12.8 %collective-permute-start.7 = (bf16[64,2048]{1,0:T(8,128)(2,1)S(1)}, bf16[64,2048]{1,0:T(8,128)(2,1)S(1)}, u32[]{:S(2)}, u32[]{:S(2)}) collective-permute-start(bf16[64,2048]{1,0:T(8,128)(2,1)S(1)} %get-tuple-element.18), channel_id=1, source_target_pairs={{0,2},{1,3},{2,0},{3,1},{4,6},{5,7},{6,4},{7,5},{8,10},{9,11},{10,... | collective-permute-start | bytes 786440 | tf_op jit(solution)/shard_map/ppermute | solution.py:250
  34.8 22.2 %collective-permute-start.10 = (bf16[64,2048]{1,0:T(8,128)(2,1)S(1)}, bf16[64,2048]{1,0:T(8,128)(2,1)S(1)}, u32[]{:S(2)}, u32[]{:S(2)}) collective-permute-start(bf16[64,2048]{1,0:T(8,128)(2,1)S(1)} %collective-permute-done.8.second), channel_id=1, source_target_pairs={{0,8},{4,12},{8,0},{12,4},{16,24},{20,28},{24,16},{28,20},{1,9},{5... | collective-permute-start | bytes 786440 | tf_op jit(solution)/shard_map/ppermute | solution.py:272
  39.9 17.1 %collective-permute-start.9 = (bf16[64,2048]{1,0:T(8,128)(2,1)S(1)}, bf16[64,2048]{1,0:T(8,128)(2,1)S(1)}, u32[]{:S(2)}, u32[]{:S(2)}) collective-permute-start(bf16[64,2048]{1,0:T(8,128)(2,1)S(1)} %collective-permute-done.7.first), channel_id=1, source_target_pairs={{0,4},{4,0},{8,12},{12,8},{16,20},{20,16},{24,28},{28,24},{1,5},{5... | collective-permute-start | bytes 786440 | tf_op jit(solution)/shard_map/ppermute | solution.py:272
  50.6 3.8 %copy-start.3 = (bf16[2,2,128,256]{3,2,1,0:T(8,128)(2,1)S(1)}, bf16[2,2,128,256]{3,2,1,0:T(8,128)(2,1)}, u32[]{:S(2)}) copy-start(bf16[2,2,128,256]{3,2,1,0:T(8,128)(2,1)} %copy-done.2) | copy-start | bytes 786436
  52.8 4.3 %collective-permute-start.11 = (bf16[128,256]{1,0:T(8,128)(2,1)S(1)}, bf16[128,256]{1,0:T(8,128)(2,1)S(1)}, u32[]{:S(2)}, u32[]{:S(2)}) collective-permute-start(bf16[128,256]{1,0:T(8,128)(2,1)S(1)} %get-tuple-element.16), channel_id=1, source_target_pairs={{0,2},{1,3},{2,0},{3,1},{4,6},{5,7},{6,4},{7,5},{8,10},{9,11},{10,... | collective-permute-start | bytes 196616 | tf_op jit(solution)/shard_map/ppermute | solution.py:250
  57.6 5.0 %collective-permute-start.12 = (bf16[128,2048]{1,0:T(8,128)(2,1)S(1)}, bf16[128,2048]{1,0:T(8,128)(2,1)S(1)}, u32[]{:S(2)}, u32[]{:S(2)}) collective-permute-start(bf16[128,2048]{1,0:T(8,128)(2,1)S(1)} %shard_map.106), channel_id=1, source_target_pairs={{0,1},{1,0},{2,3},{3,2},{4,5},{5,4},{6,7},{7,6},{8,9},{9,8},{10,11... | collective-permute-start | bytes 1572872 | tf_op jit(solution)/shard_map/ppermute | solution.py:250
  57.6 4.5 %collective-permute-start.6 = (bf16[128,256]{1,0:T(8,128)(2,1)S(1)}, bf16[128,256]{1,0:T(8,128)(2,1)S(1)}, u32[]{:S(2)}, u32[]{:S(2)}) collective-permute-start(bf16[128,256]{1,0:T(8,128)(2,1)S(1)} %get-tuple-element.15), channel_id=1, source_target_pairs={{0,2},{1,3},{2,0},{3,1},{4,6},{5,7},{6,4},{7,5},{8,10},{9,11},{10,... | collective-permute-start | bytes 196616 | tf_op jit(solution)/shard_map/ppermute | solution.py:250
  (8 other events, 7.1 us)

commit v5 on v4

--- a/solution.py
+++ b/solution.py
@@ -200,27 +200,34 @@
         values = jnp.dot(mixed[head], value_absorb[head], preferred_element_type=f32)
         parts.append(rms(values, head_gain[pl.ds(head, 1)].astype(f32)).astype(bf16))
     head_out = jnp.concatenate(parts, axis=1)
-    if outs[-1].shape[0] == rows:
+    if len(outs) == len(groups):
         for slot, out in enumerate(outs):
             out[...] = head_out[slot * rows : (slot + 1) * rows]
     else:
-        weight, out = outs
-        out[...] = jnp.dot(head_out, weight[...], preferred_element_type=f32).astype(bf16)
-
-
-def project_kernel(half, near, far, first, second, third, fourth, out):
+        weight, own_heads, core_part = outs
+        own_heads[...] = head_out[:rows]
+        core_part[...] = jnp.dot(
+            head_out[rows:], weight[...], preferred_element_type=f32
+        ).astype(bf16)
+
+
+def project_kernel(far, first, second, third, fourth, *rest):
+    near, out = rest[:-1], rest[-1]
     span = lax.axis_index("kv")
     parity = jnp.bitwise_and(jnp.bitwise_xor(span, span >> 1), 1)
-    rows = out.shape[0]
     depth = 2 * first.shape[0]
-    here = pl.ds(half * rows, rows)
     direct = jnp.concatenate([first[...], second[...]], axis=0)
     relayed = jnp.concatenate([third[...], fourth[...]], axis=0)
     at = pl.multiple_of(parity * depth, depth)
     other = pl.multiple_of((1 - parity) * depth, depth)
     partial = jnp.dot(far[:, pl.ds(at, depth)], direct, preferred_element_type=f32)
     partial += jnp.dot(far[:, pl.ds(other, depth)], relayed, preferred_element_type=f32)
-    total = near[here].astype(f32) + partial.astype(bf16).astype(f32)
+    if len(near) == 1:
+        ready = near[0][...]
+    else:
+        heads_out, weight = near
+        ready = jnp.dot(heads_out[...], weight[...], preferred_element_type=f32).astype(bf16)
+    total = ready.astype(f32) + partial.astype(bf16).astype(f32)
     out[...] = total.astype(out.dtype)
 
 
@@ -303,7 +310,7 @@
     def attend(groups, queries, grant=None, weight=()):
         return call(
             functools.partial(attend_kernel, groups),
-            shape((len(groups) * rows, model), bf16)
+            [shape((rows, heads * width), bf16), shape((rows, model), bf16)]
             if weight
             else [shape((rows, heads * width), bf16)] * len(groups),
             [SMEM] + [VMEM] * (8 + len(weight)),
@@ -319,19 +326,19 @@
     far_own, far_core = attend((2, 3), far_queries, FAR)
     far_core = swap(far_core, 2)
     far_own = swap(far_own, 2)
-    near_part = attend((0, 1), near_queries, NEAR, (out_weight,))
-
-    def project(half, far_heads, dtype):
+    near_heads, near_part = attend((0, 1), near_queries, NEAR, (out_weight,))
+
+    def project(far_heads, dtype, *near):
         return call(
-            functools.partial(project_kernel, half),
+            project_kernel,
             shape((rows, model), dtype),
-            [VMEM] * 6,
+            [VMEM] * (5 + len(near)),
             flops=2 * rows * heads * width * model,
-        )(near_part, far_heads, *far_weights)
-
-    core_part = project(1, far_core, bf16)
+        )(far_heads, *far_weights, *near)
+
+    core_part = project(far_core, bf16, near_part)
     core_part = swap(core_part, 1)
-    own_part = project(0, far_own, f32)
+    own_part = project(far_own, f32, near_heads, out_weight)
     return (own_part + core_part.astype(f32)).astype(bf16)
 
 

time: 63.9 us -> 63.4 us (level)
    all_to_all x1, starting transfers between devices: 4.47 us -> 3.77 us  [body(): lax.all_to_all(outgoing.reshape(spans, block_len, latent_width), 'kv', sp...]
    unnamed x34 -> x38, local copies, waits for them, and re-layouts: 5.76 us -> 5.77 us
where the time goes in v5:
time: 63.4 us; the launch traced here: 62.9 us
  starting transfers between devices  24 us (38%)
  waiting for transfers between devices  19.8 us (31%)
  Pallas kernels  10.7 us (17%)
  local copies, waits for them, and re-layouts  5.81 us (9%)
  matrix products  1.46 us (2%)
  other arithmetic  1 us (2%)
    ppermute x11, waiting for transfers between devices, swap(): return lax.ppermute(array, 'tp', [(i, i ^ step) for i in range(shards)])  13.4 us
    pallas_call x7, Pallas kernels, run(): pl.pallas_call(kernel, out_shape=out_shape, in_specs=in_specs, out_specs=...  10.7 us
    ppermute x11, starting transfers between devices, swap(): return lax.ppermute(array, 'tp', [(i, i ^ step) for i in range(shards)])  10.6 us
    all_to_all x1, waiting for transfers between devices, body(): lax.all_to_all(wanted, 'kv', split_axis=0, concat_axis=0, tiled=True)  6.34 us
    all_to_all x1, starting transfers between devices, body(): lax.all_to_all(wanted, 'kv', split_axis=0, concat_axis=0, tiled=True)  5.8 us
    unnamed x38, local copies, waits for them, and re-layouts  5.77 us
    ppermute x2, starting transfers between devices, relay(): return lax.ppermute(array, 'kv', [(i, i ^ step) for i in range(spans)])  3.82 us
    all_to_all x1, starting transfers between devices, body(): lax.all_to_all(outgoing.reshape(spans, block_len, latent_width), 'kv', sp...  3.77 us
  transfers between devices with their start and end apart: 15, of which 5 were waited for; matrix products, arithmetic and copies ran while one was open for 3% of the time, Pallas kernels for 16%

profile of v5, /device:TPU:0, one launch (start us, length us, event | category | flops | bytes accessed | tf_op | source)
XLA Modules:
  0.0 62.9 jit_solution(8355293113777541376)
XLA Ops:
  0.0 3.0 %collective-permute-start.1 = (bf16[128,2048]{1,0:T(8,128)(2,1)}, bf16[128,2048]{1,0:T(8,128)(2,1)}, u32[]{:S(2)}, u32[]{:S(2)}) collective-permute-start(bf16[128,2048]{1,0:T(8,128)(2,1)} %refs_0_.1), channel_id=1, source_target_pairs={{0,2},{1,3},{2,0},{3,1},{4,6},{5,7},{6,4},{7,5},{8,10},{9,11},{10,... | collective-permute-start | bytes 1572872 | tf_op jit(solution)/shard_map/ppermute | solution.py:257
  3.0 1.5 %multiply_reduce_fusion = (f32[128]{0:T(128)S(1)}, f32[128,256]{1,0:T(8,128)S(1)}) fusion(bf16[128,2048]{1,0:T(8,128)(2,1)} %refs_0_.1, bf16[2048,256]{1,0:T(8,128)(2,1)S(1)} %copy-done), kind=kOutput, calls=%fused_computation.2 | convolution fusion | flops 134283136 | bytes 1704448 | tf_op jit(solution)/shard_map/dot_general | solution.py:263
  4.7 1.3 %collective-permute-start.4 = (bf16[128,256]{1,0:T(8,128)(2,1)S(1)}, bf16[128,256]{1,0:T(8,128)(2,1)S(1)}, u32[]{:S(2)}, u32[]{:S(2)}) collective-permute-start(bf16[128,256]{1,0:T(8,128)(2,1)S(1)} %multiply_convert_fusion.own), channel_id=1, source_target_pairs={{0,2},{1,3},{2,0},{3,1},{4,6},{5,7},{6,4},{7,5},{8,10},{9,11},{10,... | collective-permute-start | bytes 196616 | tf_op jit(solution)/shard_map/ppermute | solution.py:257
  7.3 5.8 %all-to-all-start = ((s32[8,1,128]{2,1,0:T(1,128)}), s32[8,1,128]{2,1,0:T(1,128)S(1)}, u32[]{:S(2)}, u32[]{:S(2)}) async-start(s32[8,1,128]{2,1,0:T(1,128)} %shard_map.101), calls=%async_computation | async-start | bytes 8192 | tf_op jit(solution)/shard_map/all_to_all | solution.py:268
  13.1 6.3 %all-to-all-done.asked = s32[8,1,128]{2,1,0:T(1,128)S(1)} async-done(((s32[8,1,128]{2,1,0:T(1,128)}), s32[8,1,128]{2,1,0:T(1,128)S(1)}, u32[]{:S(2)}, u32[]{:S(2)}) %all-to-all-start) | async-done | bytes 4128 | tf_op jit(solution)/shard_map/all_to_all | solution.py:268
  19.5 1.4 %shard_map.102 = bf16[512,256]{1,0:T(8,128)(2,1)} custom-call(s32[8,1,128]{2,1,0:T(1,128)S(1)} %all-to-all-done.asked, bf16[128,256]{1,0:T(8,128)(2,1)S(1)} %multiply_convert_fusion.own, bf16[128,256]{1,0:T(8,128)(2,1)S(1)} %collective-permute-done.3.core, bf16[128,256]{1,0:T(8,128)(2,1)S(1)} %collective-permute-done.4.far, ...), custom_call_target="tpu_custom_call" | custom-call | bytes 786432 | tf_op jit(solution)/shard_map/pallas_call | solution.py:50
  20.9 3.8 %all-to-all-start.1 = ((bf16[8,64,256]{2,1,0:T(8,128)(2,1)}), bf16[8,64,256]{2,1,0:T(8,128)(2,1)S(1)}, u32[]{:S(2)}, u32[]{:S(2)}) async-start(bf16[8,64,256]{2,1,0:T(8,128)(2,1)} %bitcast), calls=%async_computation.1 | async-start | bytes 524288 | tf_op jit(solution)/shard_map/all_to_all | solution.py:290
  25.0 1.6 %collective-permute-start.8 = (bf16[64,2048]{1,0:T(8,128)(2,1)S(1)}, bf16[64,2048]{1,0:T(8,128)(2,1)S(1)}, u32[]{:S(2)}, u32[]{:S(2)}) collective-permute-start(bf16[64,2048]{1,0:T(8,128)(2,1)S(1)} %get-tuple-element.21), channel_id=1, source_target_pairs={{0,2},{1,3},{2,0},{3,1},{4,6},{5,7},{6,4},{7,5},{8,10},{9,11},{10,... | collective-permute-start | bytes 786440 | tf_op jit(solution)/shard_map/ppermute | solution.py:257
  27.1 7.2 %collective-permute-done.8.second = bf16[64,2048]{1,0:T(8,128)(2,1)S(1)} collective-permute-done((bf16[64,2048]{1,0:T(8,128)(2,1)S(1)}, bf16[64,2048]{1,0:T(8,128)(2,1)S(1)}, u32[]{:S(2)}, u32[]{:S(2)}) %collective-permute-start.8) | collective-permute-done | bytes 262176 | tf_op jit(solution)/shard_map/ppermute | solution.py:257
  34.3 1.8 %collective-permute-start.10 = (bf16[64,2048]{1,0:T(8,128)(2,1)S(1)}, bf16[64,2048]{1,0:T(8,128)(2,1)S(1)}, u32[]{:S(2)}, u32[]{:S(2)}) collective-permute-start(bf16[64,2048]{1,0:T(8,128)(2,1)S(1)} %collective-permute-done.8.second), channel_id=1, source_target_pairs={{0,8},{4,12},{8,0},{12,4},{16,24},{20,28},{24,16},{28,20},{1,9},{5... | collective-permute-start | bytes 786440 | tf_op jit(solution)/shard_map/ppermute | solution.py:279
  36.1 3.1 %collective-permute-done.7.first = bf16[64,2048]{1,0:T(8,128)(2,1)S(1)} collective-permute-done((bf16[64,2048]{1,0:T(8,128)(2,1)S(1)}, bf16[64,2048]{1,0:T(8,128)(2,1)S(1)}, u32[]{:S(2)}, u32[]{:S(2)}) %collective-permute-start.7) | collective-permute-done | bytes 262176 | tf_op jit(solution)/shard_map/ppermute | solution.py:257
  39.2 2.0 %collective-permute-start.9 = (bf16[64,2048]{1,0:T(8,128)(2,1)S(1)}, bf16[64,2048]{1,0:T(8,128)(2,1)S(1)}, u32[]{:S(2)}, u32[]{:S(2)}) collective-permute-start(bf16[64,2048]{1,0:T(8,128)(2,1)S(1)} %collective-permute-done.7.first), channel_id=1, source_target_pairs={{0,4},{4,0},{8,12},{12,8},{16,20},{20,16},{24,28},{28,24},{1,5},{5... | collective-permute-start | bytes 786440 | tf_op jit(solution)/shard_map/ppermute | solution.py:279
  41.2 0.8 %copy-done.17 = bf16[128,2048]{1,0:T(8,128)(2,1)} copy-done((bf16[128,2048]{1,0:T(8,128)(2,1)}, bf16[128,2048]{1,0:T(8,128)(2,1)S(1)}, u32[]{:S(2)}) %copy-start.17) | copy-done | bytes 524312
  42.0 2.9 %shard_map.100 = (bf16[2,2,128,256]{3,2,1,0:T(8,128)(2,1)S(1)}, bf16[2,2,128,256]{3,2,1,0:T(8,128)(2,1)S(1)}, s32[8,11]{1,0:T(8,128)S(1)}, bf16[2,128]{1,0:T(2,128)(2,1)S(1)}) custom-call(bf16[128,2048]{1,0:T(8,128)(2,1)} %refs_0_.1, bf16[128,2048]{1,0:T(8,128)(2,1)} %collective-permute-done.refs_1_, bf16[128,2048]{1,0:T(8,128)(2,1)} %collective-permute-done.1.refs_2_, ...), custom_call_target="tpu_custom_call" | custom-call | flops 536870912 | bytes 3803328 | tf_op jit(solution)/shard_map/pallas_call | solution.py:50
  46.3 0.8 %copy-done.4 = bf16[128,256]{1,0:T(8,128)(2,1)S(1)} copy-done((bf16[128,256]{1,0:T(8,128)(2,1)S(1)}, bf16[128,256]{1,0:T(8,128)(2,1)}, u32[]{:S(2)}) %copy-start.4) | copy-done | bytes 65560
  47.2 0.8 %copy-done.7 = bf16[128,256]{1,0:T(8,128)(2,1)S(1)} copy-done((bf16[128,256]{1,0:T(8,128)(2,1)S(1)}, bf16[128,256]{1,0:T(8,128)(2,1)}, u32[]{:S(2)}) %copy-start.7) | copy-done | bytes 65560
  48.0 0.9 %copy-done.14 = bf16[2,2,128,256]{3,2,1,0:T(8,128)(2,1)S(1)} copy-done((bf16[2,2,128,256]{3,2,1,0:T(8,128)(2,1)S(1)}, bf16[2,2,128,256]{3,2,1,0:T(8,128)(2,1)}, u32[]{:S(2)}) %copy-start.14) | copy-done | bytes 262168
  49.0 0.9 %copy-done.15 = bf16[2,256,128]{2,1,0:T(8,128)(2,1)S(1)} copy-done((bf16[2,256,128]{2,1,0:T(8,128)(2,1)S(1)}, bf16[2,256,128]{2,1,0:T(8,128)(2,1)}, u32[]{:S(2)}) %copy-start.15) | copy-done | bytes 131096
  49.9 2.2 %shard_map.103 = (bf16[128,256]{1,0:T(8,128)(2,1)S(1)}, bf16[128,256]{1,0:T(8,128)(2,1)S(1)}) custom-call(s32[8,11]{1,0:T(8,128)S(1)} %get-tuple-element.13.chosen, bf16[2,2,128,256]{3,2,1,0:T(8,128)(2,1)S(1)} %copy-done.14, bf16[128,256]{1,0:T(8,128)(2,1)S(1)} %multiply_convert_fusion.own, bf16[128,256]{1,0:T(8,128)(2,1)S(1)} %collective-permute-done.3.core, ...), custom_call_target="tpu_custom_call" | custom-call | flops 738197504 | bytes 3408384 | tf_op jit(solution)/shard_map/pallas_call | solution.py:50
  52.1 1.6 %collective-permute-start.11 = (bf16[128,256]{1,0:T(8,128)(2,1)S(1)}, bf16[128,256]{1,0:T(8,128)(2,1)S(1)}, u32[]{:S(2)}, u32[]{:S(2)}) collective-permute-start(bf16[128,256]{1,0:T(8,128)(2,1)S(1)} %get-tuple-element.19), channel_id=1, source_target_pairs={{0,2},{1,3},{2,0},{3,1},{4,6},{5,7},{6,4},{7,5},{8,10},{9,11},{10,... | collective-permute-start | bytes 196616 | tf_op jit(solution)/shard_map/ppermute | solution.py:257
  53.7 2.5 %shard_map.104 = (bf16[128,256]{1,0:T(8,128)(2,1)S(1)}, bf16[128,2048]{1,0:T(8,128)(2,1)S(1)}) custom-call(s32[8,11]{1,0:T(8,128)S(1)} %get-tuple-element.13.chosen, bf16[2,2,128,256]{3,2,1,0:T(8,128)(2,1)S(1)} %copy-done.12, bf16[128,256]{1,0:T(8,128)(2,1)S(1)} %multiply_convert_fusion.own, bf16[128,256]{1,0:T(8,128)(2,1)S(1)} %collective-permute-done.3.core, ...), custom_call_target="tpu_custom_call" | custom-call | flops 738197504 | bytes 4915712 | tf_op jit(solution)/shard_map/pallas_call | solution.py:50
  56.9 1.6 %collective-permute-start.6 = (bf16[128,256]{1,0:T(8,128)(2,1)S(1)}, bf16[128,256]{1,0:T(8,128)(2,1)S(1)}, u32[]{:S(2)}, u32[]{:S(2)}) collective-permute-start(bf16[128,256]{1,0:T(8,128)(2,1)S(1)} %get-tuple-element.16), channel_id=1, source_target_pairs={{0,2},{1,3},{2,0},{3,1},{4,6},{5,7},{6,4},{7,5},{8,10},{9,11},{10,... | collective-permute-start | bytes 196616 | tf_op jit(solution)/shard_map/ppermute | solution.py:257
  58.5 2.9 %collective-permute-done.6.far = bf16[128,256]{1,0:T(8,128)(2,1)S(1)} collective-permute-done((bf16[128,256]{1,0:T(8,128)(2,1)S(1)}, bf16[128,256]{1,0:T(8,128)(2,1)S(1)}, u32[]{:S(2)}, u32[]{:S(2)}) %collective-permute-start.6) | collective-permute-done | bytes 65568 | tf_op jit(solution)/shard_map/ppermute | solution.py:257
  62.0 0.9 %add_convert_fusion = bf16[128,2048]{1,0:T(8,128)(2,1)} fusion(f32[128,2048]{1,0:T(8,128)S(1)} %shard_map.105, bf16[128,2048]{1,0:T(8,128)(2,1)S(1)} %collective-permute-done.12), kind=kLoop, calls=%fused_computation | loop fusion | flops 786432 | bytes 2097152 | tf_op jit(solution)/shard_map/convert_element_type | solution.py:342
  (57 shorter events, 5.2 us)
Async XLA Ops:
  0.0 4.5 %copy-start.18 = (bf16[256]{0:T(256)(128)(2,1)S(1)}, bf16[256]{0:T(256)(128)(2,1)}, u32[]{:S(2)}) copy-start(bf16[256]{0:T(256)(128)(2,1)} %param.15) | copy-start | bytes 1540
  0.0 24.7 %collective-permute-start.1 = (bf16[128,2048]{1,0:T(8,128)(2,1)}, bf16[128,2048]{1,0:T(8,128)(2,1)}, u32[]{:S(2)}, u32[]{:S(2)}) collective-permute-start(bf16[128,2048]{1,0:T(8,128)(2,1)} %refs_0_.1), channel_id=1, source_target_pairs={{0,2},{1,3},{2,0},{3,1},{4,6},{5,7},{6,4},{7,5},{8,10},{9,11},{10,... | collective-permute-start | bytes 1572872 | tf_op jit(solution)/shard_map/ppermute | solution.py:257
  3.0 3.5 %copy-start.8 = (s32[8,11]{1,0:T(8,128)S(1)}, s32[8,11]{1,0:T(8,128)}, u32[]{:S(2)}) copy-start(s32[8,11]{1,0:T(8,128)} %chosen.1) | copy-start | bytes 1060
  4.5 20.5 %copy-start.1 = (bf16[256,2048]{1,0:T(8,128)(2,1)S(1)}, bf16[256,2048]{1,0:T(8,128)(2,1)}, u32[]{:S(2)}) copy-start(bf16[256,2048]{1,0:T(8,128)(2,1)} %rest_1_.1) | copy-start | bytes 3145732
  4.6 14.9 %collective-permute-start.3 = (bf16[128,256]{1,0:T(8,128)(2,1)S(1)}, bf16[128,256]{1,0:T(8,128)(2,1)S(1)}, u32[]{:S(2)}, u32[]{:S(2)}) collective-permute-start(bf16[128,256]{1,0:T(8,128)(2,1)S(1)} %multiply_convert_fusion.own), channel_id=1, source_target_pairs={{0,1},{1,0},{2,3},{3,2},{4,5},{5,4},{6,7},{7,6},{8,9},{9,8},{10,11... | collective-permute-start | bytes 196616 | tf_op jit(solution)/shard_map/ppermute | solution.py:257
  4.7 14.8 %collective-permute-start.4 = (bf16[128,256]{1,0:T(8,128)(2,1)S(1)}, bf16[128,256]{1,0:T(8,128)(2,1)S(1)}, u32[]{:S(2)}, u32[]{:S(2)}) collective-permute-start(bf16[128,256]{1,0:T(8,128)(2,1)S(1)} %multiply_convert_fusion.own), channel_id=1, source_target_pairs={{0,2},{1,3},{2,0},{3,1},{4,6},{5,7},{6,4},{7,5},{8,10},{9,11},{10,... | collective-permute-start | bytes 196616 | tf_op jit(solution)/shard_map/ppermute | solution.py:257
  5.9 13.5 %collective-permute-start.5 = (bf16[128,256]{1,0:T(8,128)(2,1)S(1)}, bf16[128,256]{1,0:T(8,128)(2,1)S(1)}, u32[]{:S(2)}, u32[]{:S(2)}) collective-permute-start(bf16[128,256]{1,0:T(8,128)(2,1)S(1)} %multiply_convert_fusion.own), channel_id=1, source_target_pairs={{0,3},{1,2},{2,1},{3,0},{4,7},{5,6},{6,5},{7,4},{8,11},{9,10},{10,... | collective-permute-start | bytes 196616 | tf_op jit(solution)/shard_map/ppermute | solution.py:257
  7.3 12.2 %all-to-all-start = ((s32[8,1,128]{2,1,0:T(1,128)}), s32[8,1,128]{2,1,0:T(1,128)S(1)}, u32[]{:S(2)}, u32[]{:S(2)}) async-start(s32[8,1,128]{2,1,0:T(1,128)} %shard_map.101), calls=%async_computation | async-start | bytes 8192 | tf_op jit(solution)/shard_map/all_to_all | solution.py:268
  13.1 28.2 %collective-permute-start = (bf16[128,2048]{1,0:T(8,128)(2,1)}, bf16[128,2048]{1,0:T(8,128)(2,1)}, u32[]{:S(2)}, u32[]{:S(2)}) collective-permute-start(bf16[128,2048]{1,0:T(8,128)(2,1)} %refs_0_.1), channel_id=1, source_target_pairs={{0,1},{1,0},{2,3},{3,2},{4,5},{5,4},{6,7},{7,6},{8,9},{9,8},{10,11... | collective-permute-start | bytes 1572872 | tf_op jit(solution)/shard_map/ppermute | solution.py:257
  20.9 25.4 %all-to-all-start.1 = ((bf16[8,64,256]{2,1,0:T(8,128)(2,1)}), bf16[8,64,256]{2,1,0:T(8,128)(2,1)S(1)}, u32[]{:S(2)}, u32[]{:S(2)}) async-start(bf16[8,64,256]{2,1,0:T(8,128)(2,1)} %bitcast), calls=%async_computation.1 | async-start | bytes 524288 | tf_op jit(solution)/shard_map/all_to_all | solution.py:290
  24.7 17.4 %copy-start.2 = (bf16[2,128,256]{2,1,0:T(8,128)(2,1)S(1)}, bf16[2,128,256]{2,1,0:T(8,128)(2,1)}, u32[]{:S(2)}) copy-start(bf16[2,128,256]{2,1,0:T(8,128)(2,1)} %refs_5_.1) | copy-start | bytes 393220
  24.7 16.6 %collective-permute-start.2 = (bf16[128,2048]{1,0:T(8,128)(2,1)}, bf16[128,2048]{1,0:T(8,128)(2,1)S(1)}, u32[]{:S(2)}, u32[]{:S(2)}) collective-permute-start(bf16[128,2048]{1,0:T(8,128)(2,1)} %collective-permute-done.1.refs_2_), channel_id=1, source_target_pairs={{0,1},{1,0},{2,3},{3,2},{4,5},{5,4},{6,7},{7,6},{8,9},{9,8},{10,11... | collective-permute-start | bytes 1572872 | tf_op jit(solution)/shard_map/ppermute | solution.py:257
  25.0 17.0 %copy-start.9 = (bf16[256]{0:T(256)(128)(2,1)S(1)}, bf16[256]{0:T(256)(128)(2,1)}, u32[]{:S(2)}) copy-start(bf16[256]{0:T(256)(128)(2,1)} %refs_6_.1) | copy-start | bytes 1540
  25.0 17.0 %copy-start.10 = (bf16[2,128]{1,0:T(2,128)(2,1)S(1)}, bf16[2,128]{1,0:T(2,128)(2,1)}, u32[]{:S(2)}) copy-start(bf16[2,128]{1,0:T(2,128)(2,1)} %refs_8_.1) | copy-start | bytes 1540
  25.0 9.2 %collective-permute-start.8 = (bf16[64,2048]{1,0:T(8,128)(2,1)S(1)}, bf16[64,2048]{1,0:T(8,128)(2,1)S(1)}, u32[]{:S(2)}, u32[]{:S(2)}) collective-permute-start(bf16[64,2048]{1,0:T(8,128)(2,1)S(1)} %get-tuple-element.21), channel_id=1, source_target_pairs={{0,2},{1,3},{2,0},{3,1},{4,6},{5,7},{6,4},{7,5},{8,10},{9,11},{10,... | collective-permute-start | bytes 786440 | tf_op jit(solution)/shard_map/ppermute | solution.py:257
  26.6 12.6 %collective-permute-start.7 = (bf16[64,2048]{1,0:T(8,128)(2,1)S(1)}, bf16[64,2048]{1,0:T(8,128)(2,1)S(1)}, u32[]{:S(2)}, u32[]{:S(2)}) collective-permute-start(bf16[64,2048]{1,0:T(8,128)(2,1)S(1)} %get-tuple-element.22), channel_id=1, source_target_pairs={{0,2},{1,3},{2,0},{3,1},{4,6},{5,7},{6,4},{7,5},{8,10},{9,11},{10,... | collective-permute-start | bytes 786440 | tf_op jit(solution)/shard_map/ppermute | solution.py:257
  34.3 21.9 %collective-permute-start.10 = (bf16[64,2048]{1,0:T(8,128)(2,1)S(1)}, bf16[64,2048]{1,0:T(8,128)(2,1)S(1)}, u32[]{:S(2)}, u32[]{:S(2)}) collective-permute-start(bf16[64,2048]{1,0:T(8,128)(2,1)S(1)} %collective-permute-done.8.second), channel_id=1, source_target_pairs={{0,8},{4,12},{8,0},{12,4},{16,24},{20,28},{24,16},{28,20},{1,9},{5... | collective-permute-start | bytes 786440 | tf_op jit(solution)/shard_map/ppermute | solution.py:279
  39.2 17.0 %collective-permute-start.9 = (bf16[64,2048]{1,0:T(8,128)(2,1)S(1)}, bf16[64,2048]{1,0:T(8,128)(2,1)S(1)}, u32[]{:S(2)}, u32[]{:S(2)}) collective-permute-start(bf16[64,2048]{1,0:T(8,128)(2,1)S(1)} %collective-permute-done.7.first), channel_id=1, source_target_pairs={{0,4},{4,0},{8,12},{12,8},{16,20},{20,16},{24,28},{28,24},{1,5},{5... | collective-permute-start | bytes 786440 | tf_op jit(solution)/shard_map/ppermute | solution.py:279
  49.9 3.8 %copy-start.5 = (bf16[128,256]{1,0:T(8,128)(2,1)S(1)}, bf16[128,256]{1,0:T(8,128)(2,1)}, u32[]{:S(2)}) copy-start(bf16[128,256]{1,0:T(8,128)(2,1)} %copy-done.3) | copy-start | bytes 196612
  49.9 3.8 %copy-start.12 = (bf16[2,2,128,256]{3,2,1,0:T(8,128)(2,1)S(1)}, bf16[2,2,128,256]{3,2,1,0:T(8,128)(2,1)}, u32[]{:S(2)}) copy-start(bf16[2,2,128,256]{3,2,1,0:T(8,128)(2,1)} %copy-done.11) | copy-start | bytes 786436
  49.9 3.8 %copy-start.16 = (bf16[2,256,128]{2,1,0:T(8,128)(2,1)S(1)}, bf16[2,256,128]{2,1,0:T(8,128)(2,1)}, u32[]{:S(2)}) copy-start(bf16[2,256,128]{2,1,0:T(8,128)(2,1)} %value_absorb.3) | copy-start | bytes 393220
  52.1 4.3 %collective-permute-start.11 = (bf16[128,256]{1,0:T(8,128)(2,1)S(1)}, bf16[128,256]{1,0:T(8,128)(2,1)S(1)}, u32[]{:S(2)}, u32[]{:S(2)}) collective-permute-start(bf16[128,256]{1,0:T(8,128)(2,1)S(1)} %get-tuple-element.19), channel_id=1, source_target_pairs={{0,2},{1,3},{2,0},{3,1},{4,6},{5,7},{6,4},{7,5},{8,10},{9,11},{10,... | collective-permute-start | bytes 196616 | tf_op jit(solution)/shard_map/ppermute | solution.py:257
  56.9 5.1 %collective-permute-start.12 = (bf16[128,2048]{1,0:T(8,128)(2,1)S(1)}, bf16[128,2048]{1,0:T(8,128)(2,1)S(1)}, u32[]{:S(2)}, u32[]{:S(2)}) collective-permute-start(bf16[128,2048]{1,0:T(8,128)(2,1)S(1)} %shard_map.106), channel_id=1, source_target_pairs={{0,1},{1,0},{2,3},{3,2},{4,5},{5,4},{6,7},{7,6},{8,9},{9,8},{10,11... | collective-permute-start | bytes 1572872 | tf_op jit(solution)/shard_map/ppermute | solution.py:257
  56.9 4.5 %collective-permute-start.6 = (bf16[128,256]{1,0:T(8,128)(2,1)S(1)}, bf16[128,256]{1,0:T(8,128)(2,1)S(1)}, u32[]{:S(2)}, u32[]{:S(2)}) collective-permute-start(bf16[128,256]{1,0:T(8,128)(2,1)S(1)} %get-tuple-element.16), channel_id=1, source_target_pairs={{0,2},{1,3},{2,0},{3,1},{4,6},{5,7},{6,4},{7,5},{8,10},{9,11},{10,... | collective-permute-start | bytes 196616 | tf_op jit(solution)/shard_map/ppermute | solution.py:257
  (10 other events, 11.5 us)
